TPU v7x, 32 devices: a whole 2x2x4 slice. The times are simulated.
32 devices in a mesh: grp: 2 (over x), ep: 16 (over z, y, core).
Axes of the slice: x: 2, y: 2, z: 4, core: 2. Of those that a mesh axis runs over, the one named last changes fastest.
Arguments:
- hidden: bfloat16 [224, 2048], P(('grp', 'ep')), parts along dimension 0, may hold values from -6 to 6
- state_in: float32 [224, 64, 4096], P(('grp', 'ep')), parts along dimension 0, may hold values from -4 to 4
- conv_state: bfloat16 [224, 3, 4608], P(('grp', 'ep')), parts along dimension 0, may hold values from -6 to 6
- expert_ids: int32 [224, 4], P(('grp', 'ep')), parts along dimension 0, may hold values from 0 to 15, as said below
- group_prob: float32 [224], P(('grp', 'ep')), parts along dimension 0, may hold values from 0.25 to 1
- expert_score: float32 [224, 4], P(('grp', 'ep')), parts along dimension 0, may hold values from 0.05 to 1
- first_gain: bfloat16 [2048], replicated, may hold values from 0.099609375 to 1.8984375
- z_weight: bfloat16 [2048, 4096], P(None, 'ep'), may hold values from -0.125 to 0.125
- x_weight: bfloat16 [2048, 4096], P(None, 'ep'), may hold values from -0.125 to 0.125
- b_weight: bfloat16 [2048, 256], replicated, may hold values from -0.125 to 0.125
- c_weight: bfloat16 [2048, 256], replicated, may hold values from -0.125 to 0.125
- dt_weight: bfloat16 [2048, 64], replicated, may hold values from -0.125 to 0.125
- conv_weight: bfloat16 [4, 4608], replicated, may hold values from -3 to 3
- conv_bias: bfloat16 [4608], replicated, may hold values from -3 to 3
- dt_bias: float32 [64], replicated, may hold values from -4 to 0
- decay_log: float32 [64], replicated, may hold values from 0 to 2
- skip_gain: float32 [64], replicated, may hold values from 0.1 to 1.9
- inner_gain: bfloat16 [4096], replicated, may hold values from 0.099609375 to 1.8984375
- out_weight: bfloat16 [4096, 2048], P(None, 'ep'), may hold values from -0.09375 to 0.09375
- second_gain: bfloat16 [2048], replicated, may hold values from 0.099609375 to 1.8984375
- expert_gate: bfloat16 [16, 2048, 512], P('ep'), may hold values from -0.125 to 0.125
- expert_up: bfloat16 [16, 2048, 512], P('ep'), may hold values from -0.125 to 0.125
- expert_down: bfloat16 [16, 512, 2048], P('ep'), may hold values from -0.25 to 0.25
Outputs:
- layer_out: bfloat16 [224, 2048], P(('grp', 'ep')), parts along dimension 0
- state_out: float32 [224, 64, 4096], P(('grp', 'ep')), parts along dimension 0
- conv_out: bfloat16 [224, 3, 4608], P(('grp', 'ep')), parts along dimension 0
There are 2 independent parts, one for each index of `grp`. A program takes and returns all parts, laid end to end along the dimension named above; an argument that names none is the same for every part. Nothing has to cross between parts.
Inputs may be any that keep to these rules, and one draw needn't show every extreme that they name: `expert_ids`: each row names 4 different experts of one expert group (numbers g * 8 to g * 8 + 7). Among the 7 rows of one device no expert is named more than 3 times, and in every draw one expert is named exactly 3 times by the rows of every device.
All inputs are finite; a program needn't handle non-finite values.
Results may differ from a plain program's by a relative error of at most 0.014.
Values may be sent and summed in bfloat16 or wider, within the bound.
A program may use at most 128 MiB of HBM per device.

v0:
```python
import functools

import jax
import jax.numpy as jnp
from jax import lax
from jax.experimental import pallas as pl
from jax.experimental.pallas import tpu as pltpu
from jax.sharding import PartitionSpec as P

HEADS = 64
HEAD_DIM = 64
SSM_GROUPS = 4
STATE = 64
TOP = 4
EPS = 1e-06
MESH = pl.DeviceIdType.MESH
F32 = jnp.float32
BF16 = jnp.bfloat16
ROWS = 8


def rms_scale(values, gain_vec):
    return (
        values
        * lax.rsqrt(jnp.mean(values * values, axis=-1, keepdims=True) + EPS)
        * gain_vec.astype(F32)
    )


def peer(index):
    return (lax.axis_index("grp"), index)


def enter(n):
    me = lax.axis_index("ep")
    barrier = pltpu.get_barrier_semaphore()

    for d in range(1, n):
        pl.semaphore_signal(
            barrier, inc=1, device_id=peer(lax.rem(me + d, n)), device_id_type=MESH
        )
    pl.semaphore_wait(barrier, n - 1)


def remote(src, dst, send_sem, recv_sem, index):
    return pltpu.make_async_remote_copy(
        src_ref=src,
        dst_ref=dst,
        send_sem=send_sem,
        recv_sem=recv_sem,
        device_id=peer(index),
        device_id_type=MESH,
    )


def gather_start(n, src, buf, send, recv):
    me = lax.axis_index("ep")
    copies = []
    for d in range(1, n // 4):
        copy = remote(src, buf.at[me], send.at[d - 1], recv.at[d - 1], lax.rem(me + 4 * d, n))
        copy.start()
        copies.append(copy)
    return copies


def gather_finish(n, src, buf, send, recv, copies):
    me = lax.axis_index("ep")
    outer = n // 4
    core = lax.rem(me, 2)
    mid = lax.rem(me // 2, 2)
    mate = me + 1 - 2 * core
    across = me + 2 - 4 * mid
    second, third, fourth = [], [], []
    base = outer - 1
    for d in range(outer):
        block = lax.rem(me + n - 4 * d, n)
        if d > 0:
            copies[d - 1].wait_recv()
        piece = src if d == 0 else buf.at[block]
        copy = remote(piece, buf.at[block], send.at[base + d], recv.at[base + d], across)
        copy.start()
        second.append(copy)
        copy = remote(
            piece, buf.at[block], send.at[base + outer + d], recv.at[base + outer + d], mate
        )
        copy.start()
        third.append(copy)
    for d in range(outer):
        block = lax.rem(across + n - 4 * d, n)
        second[d].wait_recv()
        slot = base + 2 * outer + d
        copy = remote(buf.at[block], buf.at[block], send.at[slot], recv.at[slot], mate)
        copy.start()
        fourth.append(copy)
    for copy in third + fourth:
        copy.wait_recv()
    for copy in copies + second + third + fourth:
        copy.wait_send()


def exchange_start(n, out_buf, in_buf, send, recv):
    me = lax.axis_index("ep")
    copies = []
    for d in range(1, n):
        to = lax.rem(me + d, n)
        copy = remote(out_buf.at[to], in_buf.at[me], send.at[d - 1], recv.at[d - 1], to)
        copy.start()
        copies.append(copy)
    in_buf[me] = out_buf[me]
    return copies


def spread(ref):
    value = ref[...].astype(F32)
    return jnp.concatenate([value[i : i + 1] for i in range(value.shape[0])], axis=1)


def column(row):
    size = row.shape[1]
    at = lax.broadcasted_iota(jnp.int32, (size, size), 0)
    to = lax.broadcasted_iota(jnp.int32, (size, size), 1)
    return jnp.sum(jnp.where(at == to, row, jnp.zeros_like(row)), axis=1, keepdims=True)


def project_kernel(
    n,
    own_ref,
    ids_ref,
    gain_ref,
    z_any,
    x_any,
    b_any,
    c_any,
    dt_any,
    all_ref,
    z_ref,
    x_ref,
    bc_ref,
    dt_ref,
    hid_ref,
    hbuf,
    normed,
    zw,
    xw,
    bw,
    cw,
    dw,
    out_buf,
    in_buf,
    wsem,
    gs,
    gr,
    xs,
    xr,
    zs,
    zr,
):
    loads = [
        pltpu.make_async_copy(src, dst, wsem.at[i])
        for i, (src, dst) in enumerate(
            [(b_any, bw), (c_any, cw), (dt_any, dw), (z_any, zw), (x_any, xw)]
        )
    ]
    for load in loads:
        load.start()
    rows, width = own_ref.shape
    ids = ids_ref[...].astype(F32)
    pick = lax.broadcasted_iota(jnp.int32, (TOP, 128), 0)
    lane = lax.broadcasted_iota(jnp.int32, (TOP, 128), 1)
    spot = jnp.zeros((TOP, 128), F32)
    for r in range(rows):
        spot = spot + jnp.where(lane == TOP * r + pick, ids[:, r : r + 1] + 1.0, 0.0)
    id_row = jnp.sum(spot, axis=0, keepdims=True) - 1.0
    id_row = jnp.concatenate([id_row, jnp.full((1, width - 128), -1.0, F32)], axis=1)
    hid_ref[...] = jnp.concatenate([own_ref[...].astype(F32), id_row], axis=0).astype(BF16)
    enter(n)
    me = lax.axis_index("ep")
    copies = gather_start(n, hid_ref, hbuf, gs, gr)
    hbuf[me] = hid_ref[...]
    gain = spread(gain_ref)
    mine = rms_scale(hid_ref[...].astype(F32), gain).astype(BF16)
    for load in loads[:3]:
        load.wait()
    span = bw.shape[1]
    bc_ref[:, :span] = jnp.dot(mine, bw[...], preferred_element_type=F32).astype(BF16).astype(F32)
    bc_ref[:, span:] = jnp.dot(mine, cw[...], preferred_element_type=F32).astype(BF16).astype(F32)
    dt = lax.dot_general(mine, dw[...], (((1,), (1,)), ((), ())), preferred_element_type=F32)
    dt_ref[...] = dt.astype(BF16).astype(F32)
    gather_finish(n, hid_ref, hbuf, gs, gr, copies)
    for j in range(0, n, 2):
        pair = jnp.concatenate([hbuf[j].astype(F32), hbuf[j + 1].astype(F32)], axis=0)
        all_ref[j * ROWS : (j + 2) * ROWS, :] = pair.astype(BF16)
        normed[j * ROWS : (j + 2) * ROWS, :] = rms_scale(pair, gain).astype(BF16)
    for load in loads[3:]:
        load.wait()
    cols = zw.shape[1]
    flights = []
    for h, (weight, send, recv) in enumerate([(xw, xs, xr), (zw, zs, zr)]):
        part = jnp.dot(normed[...], weight[...], preferred_element_type=F32)
        for j in range(n):
            out_buf[h, j] = part[j * ROWS : (j + 1) * ROWS].astype(BF16)
        flights.append(exchange_start(n, out_buf.at[h], in_buf.at[h], send, recv))
    for h, ref in enumerate([x_ref, z_ref]):
        for copy in flights[h]:
            copy.wait_recv()
        for j in range(n):
            ref[:, j * cols : (j + 1) * cols] = in_buf[h, j].astype(F32)
    for copy in flights[0] + flights[1]:
        copy.wait_send()


def project(n, hidden, ids, first_gain, z_weight, x_weight, b_weight, c_weight, dt_weight):
    width = hidden.shape[1]
    cols = z_weight.shape[1]
    inner = n * cols
    span = b_weight.shape[1]
    vm = pl.BlockSpec(memory_space=pltpu.VMEM)
    hbm = pl.BlockSpec(memory_space=pl.ANY)
    dma = pltpu.SemaphoreType.DMA
    return pl.pallas_call(
        functools.partial(project_kernel, n),
        out_shape=(
            jax.ShapeDtypeStruct((n * ROWS, width), BF16),
            jax.ShapeDtypeStruct((ROWS, inner), F32),
            jax.ShapeDtypeStruct((ROWS, inner), F32),
            jax.ShapeDtypeStruct((ROWS, 2 * span), F32),
            jax.ShapeDtypeStruct((ROWS, dt_weight.shape[0]), F32),
        ),
        in_specs=[vm] * 3 + [hbm] * 5,
        out_specs=(vm,) * 5,
        scratch_shapes=[
            pltpu.VMEM((ROWS, width), BF16),
            pltpu.VMEM((n, ROWS, width), BF16),
            pltpu.VMEM((n * ROWS, width), BF16),
            pltpu.VMEM(z_weight.shape, BF16),
            pltpu.VMEM(x_weight.shape, BF16),
            pltpu.VMEM(b_weight.shape, BF16),
            pltpu.VMEM(c_weight.shape, BF16),
            pltpu.VMEM(dt_weight.shape, BF16),
            pltpu.VMEM((2, n, ROWS, cols), BF16),
            pltpu.VMEM((2, n, ROWS, cols), BF16),
            dma((5,)),
        ]
        + [dma((n - 1,))] * 6,
        compiler_params=pltpu.CompilerParams(
            collective_id=0, has_side_effects=True, vmem_limit_bytes=60 << 20
        ),
        name="project",
    )(hidden, ids.T, first_gain.reshape(-1, 128), z_weight, x_weight, b_weight, c_weight, dt_weight)


def state_kernel(heads_ref, bc_ref, par_ref, gain_ref, st_ref, out_ref, y_ref):
    s = pl.program_id(0)
    heads = heads_ref[0]
    x = heads[:, :HEAD_DIM]
    z = heads[:, HEAD_DIM : 2 * HEAD_DIM]
    dt = heads[:, 2 * HEAD_DIM : 2 * HEAD_DIM + 1]
    par = par_ref[...]
    step = jax.nn.softplus(dt + par[:, 0:1])
    decay = jnp.exp(-step * jnp.exp(par[:, 1:2]))
    sx = step * x
    sx = jnp.concatenate([sx, sx], axis=1)
    row = bc_ref[pl.ds(s, 1), :]
    span = SSM_GROUPS * STATE
    per = HEADS // SSM_GROUPS
    bs, cs = [], []
    for g in range(SSM_GROUPS):
        b = row[:, g * STATE : (g + 1) * STATE]
        c = row[:, span + g * STATE : span + (g + 1) * STATE]
        bs.append(jnp.broadcast_to(jnp.concatenate([b, b], axis=1), (per, 2 * STATE)))
        cs.append(jnp.broadcast_to(jnp.concatenate([c, c], axis=1), (per, 2 * STATE)))
    b_all = jnp.concatenate(bs, axis=0)
    c_all = jnp.concatenate(cs, axis=0)
    decay = jnp.broadcast_to(decay, (HEADS, 128))
    half = lax.broadcasted_iota(jnp.int32, (HEADS, 128), 1) // STATE
    blocks = HEAD_DIM * STATE // 256
    k_of = lax.broadcasted_iota(jnp.int32, (256, 128), 0) // STATE
    l_of = lax.broadcasted_iota(jnp.int32, (256, 128), 1)
    fold = (k_of == l_of).astype(F32).astype(BF16)
    prods = []
    for k in range(blocks):
        parts = []
        for i in range(2):
            lane = (2 * k + i) * 128
            grown = jnp.take_along_axis(sx, half + (4 * k + 2 * i), axis=1)
            new = decay * st_ref[0, :, lane : lane + 128] + grown * b_all
            out_ref[0, :, lane : lane + 128] = new
            parts.append((new * c_all).astype(BF16))
        prods.append(jnp.concatenate(parts, axis=1))
    sums = jnp.dot(jnp.concatenate(prods, axis=0), fold, preferred_element_type=F32)
    total = sums[:HEADS]
    for k in range(1, blocks):
        total = total + pltpu.roll(sums[k * HEADS : (k + 1) * HEADS], 4 * k, 1)
    readout = total[:, :HEAD_DIM] + par[:, 2:3] * x
    gated = readout * jax.nn.silu(z)
    mean = jnp.sum(gated * gated, keepdims=True) / (HEADS * HEAD_DIM)
    y_ref[0] = gated * lax.rsqrt(mean + EPS) * gain_ref[...]


def state_update(heads, bc, par, gain, state_in):
    rows, _, flat = state_in.shape
    return pl.pallas_call(
        state_kernel,
        grid=(rows,),
        out_shape=(
            jax.ShapeDtypeStruct(state_in.shape, F32),
            jax.ShapeDtypeStruct((rows, HEADS, HEAD_DIM), F32),
        ),
        in_specs=[
            pl.BlockSpec((1,) + heads.shape[1:], lambda s: (s, 0, 0)),
            pl.BlockSpec(bc.shape, lambda s: (0, 0)),
            pl.BlockSpec(par.shape, lambda s: (0, 0)),
            pl.BlockSpec(gain.shape, lambda s: (0, 0)),
            pl.BlockSpec((1, HEADS, flat), lambda s: (s, 0, 0)),
        ],
        out_specs=(
            pl.BlockSpec((1, HEADS, flat), lambda s: (s, 0, 0)),
            pl.BlockSpec((1, HEADS, HEAD_DIM), lambda s: (s, 0, 0)),
        ),
        compiler_params=pltpu.CompilerParams(vmem_limit_bytes=40 << 20),
        name="state",
    )(heads, bc, par, gain, state_in)


def expert_kernel(
    n,
    cap,
    y_ref,
    hid_ref,
    own_ref,
    ids_ref,
    prob_ref,
    score_ref,
    gain_ref,
    ow_any,
    eg_any,
    eu_any,
    ed_any,
    out_ref,
    ybuf,
    yflat,
    pbuf,
    mixed,
    normed,
    act,
    eo,
    ow,
    eg,
    eu,
    ed,
    out_buf,
    in_buf,
    wsem,
    ys,
    yr,
    ps,
    pr,
    es,
    er,
    fs,
    fr,
):
    loads = [
        pltpu.make_async_copy(src, dst, wsem.at[i])
        for i, (src, dst) in enumerate(
            [(ow_any, ow), (eg_any.at[0], eg), (eu_any.at[0], eu), (ed_any.at[0], ed)]
        )
    ]
    for load in loads:
        load.start()
    enter(n)
    me = lax.axis_index("ep")
    total = n * ROWS
    copies = gather_start(n, y_ref, ybuf, ys, yr)
    ybuf[me] = y_ref[...]
    q = lax.broadcasted_iota(jnp.int32, (total, total), 0)
    t = lax.broadcasted_iota(jnp.int32, (total, total), 1)
    last = (t == (q // ROWS) * ROWS + (ROWS - 1)).astype(F32).astype(BF16)
    ids = jnp.dot(last, hid_ref[:, :128], preferred_element_type=F32)
    flags = (ids == me.astype(F32)).astype(F32).astype(BF16)
    lane = lax.broadcasted_iota(jnp.int32, (128, total), 0) // TOP
    token = lax.rem(lax.broadcasted_iota(jnp.int32, (128, total), 1), ROWS)
    here = jnp.dot(flags, (lane == token).astype(F32).astype(BF16), preferred_element_type=F32)
    before = jnp.dot(flags, (lane < token).astype(F32).astype(BF16), preferred_element_type=F32)
    slot = lax.rem(q, ROWS).astype(F32)
    chosen = (q // ROWS == t // ROWS) & (here > 0.5) & (before == slot)
    select = chosen.astype(F32).astype(BF16)
    rows = out_ref.shape[0]
    col = lax.broadcasted_iota(jnp.int32, (rows, n * cap), 1)
    score = score_ref[...]
    share = prob_ref[...] * score / jnp.sum(score, axis=0, keepdims=True)
    ids = ids_ref[...].astype(F32)
    weight = jnp.zeros((rows, n * cap), F32)
    used = jnp.zeros((rows, n * cap), F32)
    for pick in range(TOP):
        hit = (column(ids[pick : pick + 1]) == (col // cap).astype(F32)).astype(F32)
        used = used + hit
        weight = weight + hit * column(share[pick : pick + 1])
    row_id = lax.broadcasted_iota(jnp.int32, (rows, n * cap), 0)
    rank = jnp.zeros((rows, n * cap), F32)
    for r in range(rows - 1):
        rank = rank + jnp.where(row_id > r, used[r : r + 1, :], 0.0)
    weight = jnp.where(rank == lax.rem(col, cap).astype(F32), weight, 0.0)
    high = weight.astype(BF16)
    low = (weight - high.astype(F32)).astype(BF16)
    gather_finish(n, y_ref, ybuf, ys, yr, copies)
    for j in range(0, n, 2):
        pair = jnp.concatenate([ybuf[j].astype(F32), ybuf[j + 1].astype(F32)], axis=0)
        yflat[j * ROWS : (j + 2) * ROWS, :] = pair.astype(BF16)
    loads[0].wait()
    pbuf[me] = jnp.dot(yflat[...], ow[...], preferred_element_type=F32).astype(BF16)
    copies = gather_start(n, pbuf.at[me], pbuf, ps, pr)
    gather_finish(n, pbuf.at[me], pbuf, ps, pr, copies)
    cols = pbuf.shape[2]
    for j in range(n):
        at = slice(j * cols, (j + 1) * cols)
        mixed[:, at] = (hid_ref[:, at].astype(F32) + pbuf[j].astype(F32)).astype(BF16)
    gain = spread(gain_ref)
    for j in range(0, total, 16):
        normed[j : j + 16, :] = rms_scale(mixed[j : j + 16, :].astype(F32), gain).astype(BF16)
    for load in loads[1:]:
        load.wait()
    for j in range(0, eg.shape[1], 256):
        at = slice(j, j + 256)
        gate = jnp.dot(normed[...], eg[:, at], preferred_element_type=F32)
        up = jnp.dot(normed[...], eu[:, at], preferred_element_type=F32)
        act[:, at] = (jax.nn.silu(gate) * up).astype(BF16)
    width = eo.shape[1]
    wide = width // 2
    tile = 256

    def down(i, carry):
        at = pl.ds(pl.multiple_of(i * tile, tile), tile)
        part = jnp.dot(act[...], ed[:, at], preferred_element_type=F32).astype(BF16)
        eo[:, at] = jnp.dot(select, part, preferred_element_type=F32)
        return carry

    flights = []
    for h, (send, recv) in enumerate([(es, er), (fs, fr)]):
        lax.fori_loop(h * wide // tile, (h + 1) * wide // tile, down, 0)
        for j in range(n):
            out_buf[h, j] = eo[j * ROWS : j * ROWS + cap, h * wide : (h + 1) * wide].astype(BF16)
        flights.append(exchange_start(n, out_buf.at[h], in_buf.at[h], send, recv))
    start = pl.multiple_of(me * ROWS, ROWS)
    eo[...] = mixed[...].astype(F32)
    base = eo[pl.ds(start, ROWS), :][:rows]
    per = ROWS // cap
    for h in range(2):
        for copy in flights[h]:
            copy.wait_recv()
        for j in range(0, n, per):
            eo[j * cap : (j + per) * cap, :wide] = jnp.concatenate(
                [in_buf[h, j + i].astype(F32) for i in range(per)], axis=0
            )
        back = eo[: n * cap, :wide].astype(BF16)
        moe = jnp.dot(high, back, preferred_element_type=F32) + jnp.dot(
            low, back, preferred_element_type=F32
        )
        at = slice(h * wide, (h + 1) * wide)
        out_ref[:, at] = (base[:, at] + moe).astype(BF16)
    for copy in flights[0] + flights[1]:
        copy.wait_send()


def experts(
    n, cap, y8, hid_all, hidden, ids, prob, score, second_gain, out_weight, gate_w, up_w, down_w
):
    total, width = hid_all.shape
    inner = y8.shape[1]
    cols = out_weight.shape[1]
    hid_units = gate_w.shape[2]
    vm = pl.BlockSpec(memory_space=pltpu.VMEM)
    hbm = pl.BlockSpec(memory_space=pl.ANY)
    dma = pltpu.SemaphoreType.DMA
    return pl.pallas_call(
        functools.partial(expert_kernel, n, cap),
        out_shape=jax.ShapeDtypeStruct(hidden.shape, BF16),
        in_specs=[vm] * 7 + [hbm] * 4,
        out_specs=vm,
        scratch_shapes=[
            pltpu.VMEM((n, ROWS, inner), BF16),
            pltpu.VMEM((total, inner), BF16),
            pltpu.VMEM((n, total, cols), BF16),
            pltpu.VMEM((total, width), BF16),
            pltpu.VMEM((total, width), BF16),
            pltpu.VMEM((total, hid_units), BF16),
            pltpu.VMEM((total, width), F32),
            pltpu.VMEM(out_weight.shape, BF16),
            pltpu.VMEM(gate_w.shape[1:], BF16),
            pltpu.VMEM(up_w.shape[1:], BF16),
            pltpu.VMEM(down_w.shape[1:], BF16),
            pltpu.VMEM((2, n, cap, width // 2), BF16),
            pltpu.VMEM((2, n, cap, width // 2), BF16),
            dma((4,)),
        ]
        + [dma((n - 1,))] * 8,
        compiler_params=pltpu.CompilerParams(
            collective_id=1, has_side_effects=True, vmem_limit_bytes=60 << 20
        ),
        name="experts",
    )(
        y8,
        hid_all,
        hidden,
        ids.T,
        prob[None, :],
        score.T,
        second_gain.reshape(-1, 128),
        out_weight,
        gate_w,
        up_w,
        down_w,
    )


def body(
    hidden,
    state_in,
    conv_state,
    expert_ids,
    group_prob,
    expert_score,
    first_gain,
    z_weight,
    x_weight,
    b_weight,
    c_weight,
    dt_weight,
    conv_weight,
    conv_bias,
    dt_bias,
    decay_log,
    skip_gain,
    inner_gain,
    out_weight,
    second_gain,
    expert_gate,
    expert_up,
    expert_down,
):
    n = lax.axis_size("ep")
    rows, width = hidden.shape
    inner = HEADS * HEAD_DIM
    hid_all, z8, x8, bc8, dt8 = project(
        n, hidden, expert_ids, first_gain, z_weight, x_weight, b_weight, c_weight, dt_weight.T
    )
    fresh = jnp.concatenate([x8[:rows], bc8[:rows]], axis=1).astype(BF16)
    taps = conv_weight.astype(F32)
    held = conv_state.shape[1]
    summed = jnp.sum(conv_state.astype(F32) * taps[None, :held], axis=1)
    summed = summed + fresh.astype(F32) * taps[held][None]
    conv_out = jnp.concatenate([conv_state[:, 1:], fresh[:, None, :]], axis=1)
    active = jax.nn.silu(summed + conv_bias.astype(F32)[None, :])
    heads = jnp.concatenate(
        [
            active[:, :inner].reshape(rows, HEADS, HEAD_DIM),
            z8[:rows].reshape(rows, HEADS, HEAD_DIM),
            dt8[:rows][:, :, None],
        ],
        axis=2,
    )
    par = jnp.stack([dt_bias, decay_log, skip_gain], axis=1)
    state_out, y_heads = state_update(
        heads,
        active[:, inner:],
        par,
        inner_gain.astype(F32).reshape(HEADS, HEAD_DIM),
        state_in,
    )
    y8 = jnp.pad(y_heads.astype(BF16).reshape(rows, inner), ((0, ROWS - rows), (0, 0)))
    need = max(2, (3 * rows * TOP + 2 * n - 1) // (2 * n))
    cap = 2 if need <= 2 else 4 if need <= 4 else 8
    layer_out = experts(
        n,
        cap,
        y8,
        hid_all,
        hidden,
        expert_ids,
        group_prob,
        expert_score,
        second_gain,
        out_weight,
        expert_gate,
        expert_up,
        expert_down,
    )
    return (layer_out, state_out, conv_out)


def solution(mesh):
    in_specs = (
        P(("grp", "ep"), None),
        P(("grp", "ep"), None, None),
        P(("grp", "ep"), None, None),
        P(("grp", "ep"), None),
        P(("grp", "ep")),
        P(("grp", "ep"), None),
        P(),
        P(None, "ep"),
        P(None, "ep"),
        P(),
        P(),
        P(),
        P(),
        P(),
        P(),
        P(),
        P(),
        P(),
        P(None, "ep"),
        P(),
        P("ep", None, None),
        P("ep", None, None),
        P("ep", None, None),
    )
    out_specs = (P(("grp", "ep"), None), P(("grp", "ep"), None, None), P(("grp", "ep"), None, None))
    return jax.shard_map(body, mesh=mesh, in_specs=in_specs, out_specs=out_specs, check_vma=False)
```

profile of v0, /device:TPU:0, one launch (start us, length us, event | category | flops | bytes accessed | tf_op | source)
XLA Modules:
  0.0 78.6 jit_solution(9900848179019110526)
XLA Ops:
  0.6 0.0 copy-start.2
  0.6 0.0 copy-start.1
  0.7 0.0 copy-start.6
  0.7 23.3 %project.1 = (bf16[128,2048]{1,0:T(8,128)(2,1)}, f32[8,4096]{1,0:T(8,128)}, f32[8,4096]{1,0:T(8,128)}, f32[8,512]{1,0:T(8,128)}, f32[8,64]{1,0:T(8,128)}) custom-call(bf16[7,2048]{1,0:T(8,128)(2,1)} %own_ref.3, s32[4,7]{1,0:T(4,128)} %bitcast.18, bf16[16,128]{1,0:T(8,128)(2,1)} %bitcast.20, bf16[2048,256]{1,0:T(8,128)(2,1)} %z_any.1, ...), custom_call_target="tpu_custom_call" | custom-call | tf_op jit(solution)/shard_map/project/pallas_call | solution.py:220
  23.9 0.0 copy-start.4
  23.9 0.0 copy-start.8
  24.0 0.0 copy-start.9
  24.0 0.0 copy-start.10
  24.0 0.0 copy-start.7
  24.0 1.0 %slice.44 = bf16[7,4096]{1,0:T(8,128)(2,1)S(1)} slice(f32[8,4096]{1,0:T(8,128)} %get-tuple-element.10), slice={[0:7], [0:4096]} | slice | bytes 114688 | tf_op jit(solution)/shard_map/slice | solution.py:547
  25.0 0.7 slice.45
  25.7 0.1 multiply_reduce_fusion
  25.8 0.1 slice_reduce_fusion
  25.9 0.1 divide_multiply_fusion
  26.0 0.1 reshape.60
  26.1 0.7 slice_bitcast_fusion
  26.7 0.1 copy.33
  26.9 0.0 copy-done.4
  26.9 0.1 reshape.61
  27.0 0.2 pad_maximum_fusion.heads_ref
  27.2 0.0 copy-done.8
  27.2 0.0 copy-done.9
  27.2 0.0 copy-done.10
  27.3 0.1 copy.34.par_ref
  27.4 0.1 reshape.67.gain_ref
  27.4 3.1 %copy-done = f32[7,64,4096]{2,1,0:T(8,128)S(1)} copy-done((f32[7,64,4096]{2,1,0:T(8,128)S(1)}, f32[7,64,4096]{2,1,0:T(8,128)}, u32[]{:S(2)}) %copy-start) | copy-done | bytes 7340056
  30.5 8.0 %state.1 = (f32[7,64,4096]{2,1,0:T(8,128)}, f32[7,64,64]{2,1,0:T(8,128)S(1)}) custom-call(f32[7,64,129]{2,1,0:T(8,128)S(1)} %pad_maximum_fusion.heads_ref, f32[7,512]{1,0:T(8,128)S(1)} %slice.39.bc_ref, f32[64,3]{1,0:T(8,128)S(1)} %copy.34.par_ref, f32[64,64]{1,0:T(8,128)S(1)} %reshape.67.gain_ref, f32[7,64,4096]{2,1,0:T(8,128)S(1)} %copy-done), custom_call_target="tpu_custom_call" | custom-call | tf_op jit(solution)/shard_map/state/pallas_call | solution.py:302
  38.6 0.1 reshape.64
  38.7 0.6 pad.4.y_ref
  39.4 37.0 %experts.1 = bf16[7,2048]{1,0:T(8,128)(2,1)} custom-call(bf16[8,4096]{1,0:T(8,128)(2,1)} %pad.4.y_ref, bf16[128,2048]{1,0:T(8,128)(2,1)} %get-tuple-element.15.hid_ref, bf16[7,2048]{1,0:T(8,128)(2,1)} %own_ref.3, s32[4,7]{1,0:T(4,128)} %bitcast.19, f32[1,7]{1,0:T(1,128)} %bitcast.23, f32[4,7]{1,0:T(4,128)} %bitcast.22, bf16[16,128]{1,0:T(8,128)(2,1)} %bitcast.21, ...), custom_call_target="tpu_custom_call" | custom-call | tf_op jit(solution)/shard_map/experts/pallas_call | solution.py:475
  76.5 0.7 maximum_maximum_fusion
  77.2 1.4 %copy.36 = bf16[7,2048]{1,0:T(8,128)(2,1)} copy(bf16[7,2048]{1,0:T(8,128)(2,1)} %experts.1) | data formatting | bytes 57344
  (20 shorter events, 0.1 us)
Async XLA Ops:
  0.6 25.1 %copy-start.2 = (bf16[4,4608]{1,0:T(4,128)(2,1)S(1)}, bf16[4,4608]{1,0:T(4,128)(2,1)}, u32[]{:S(2)}) copy-start(bf16[4,4608]{1,0:T(4,128)(2,1)} %param.35) | copy-start | bytes 110596
  0.6 25.1 %copy-start.1 = (bf16[7,3,4608]{2,0,1:T(8,128)(2,1)S(1)}, bf16[7,3,4608]{2,0,1:T(8,128)(2,1)}, u32[]{:S(2)}) copy-start(bf16[7,3,4608]{2,0,1:T(8,128)(2,1)} %param.25) | copy-start | bytes 580612
  0.7 25.2 %copy-start.6 = (bf16[4608]{0:T(1024)(128)(2,1)S(1)}, bf16[4608]{0:T(1024)(128)(2,1)}, u32[]{:S(2)}) copy-start(bf16[4608]{0:T(1024)(128)(2,1)} %param.36) | copy-start | bytes 27652
  23.9 3.0 %copy-start.4 = (f32[8,4096]{1,0:T(8,128)S(1)}, f32[8,4096]{1,0:T(8,128)}, u32[]{:S(2)}) copy-start(f32[8,4096]{1,0:T(8,128)} %get-tuple-element.12) | copy-start | bytes 393220
  23.9 3.3 %copy-start.8 = (f32[64]{0:T(128)S(1)}, f32[64]{0:T(128)}, u32[]{:S(2)}) copy-start(f32[64]{0:T(128)} %param.39) | copy-start | bytes 772
  24.0 3.3 %copy-start.9 = (f32[64]{0:T(128)S(1)}, f32[64]{0:T(128)}, u32[]{:S(2)}) copy-start(f32[64]{0:T(128)} %param.38) | copy-start | bytes 772
  24.0 3.3 %copy-start.10 = (f32[64]{0:T(128)S(1)}, f32[64]{0:T(128)}, u32[]{:S(2)}) copy-start(f32[64]{0:T(128)} %param.37) | copy-start | bytes 772
  24.0 3.4 %copy-start.7 = (bf16[4096]{0:T(1024)(128)(2,1)S(1)}, bf16[4096]{0:T(1024)(128)(2,1)}, u32[]{:S(2)}) copy-start(bf16[4096]{0:T(1024)(128)(2,1)} %param.40) | copy-start | bytes 24580
  27.4 3.1 %copy-start = (f32[7,64,4096]{2,1,0:T(8,128)S(1)}, f32[7,64,4096]{2,1,0:T(8,128)}, u32[]{:S(2)}) copy-start(f32[7,64,4096]{2,1,0:T(8,128)} %st_ref.1) | copy-start | bytes 22020100
  39.4 37.1 %copy-start.3 = (f32[8,4096]{1,0:T(8,128)S(1)}, f32[8,4096]{1,0:T(8,128)}, u32[]{:S(2)}) copy-start(f32[8,4096]{1,0:T(8,128)} %get-tuple-element.10) | copy-start | bytes 393220
  39.4 37.1 %copy-start.5 = (f32[8,512]{1,0:T(8,128)S(1)}, f32[8,512]{1,0:T(8,128)}, u32[]{:S(2)}) copy-start(f32[8,512]{1,0:T(8,128)} %get-tuple-element.11) | copy-start | bytes 49156
  39.4 37.1 %slice-start = ((bf16[7,3,4608]{2,0,1:T(8,128)(2,1)}), bf16[7,2,4608]{2,0,1:T(8,128)(2,1)S(1)}, s32[]{:S(2)}) async-start(bf16[7,3,4608]{2,0,1:T(8,128)(2,1)} %param.25), calls=%async_computation | async-start | bytes 294912 | tf_op jit(solution)/shard_map/slice | solution.py:552
where the time goes:
time: 78.9 us; the launch traced here: 78.6 us
  Pallas kernels  68.3 us (87%)
  local copies, waits for them, and re-layouts  8.27 us (10%)
  other arithmetic  1.09 us (1%)
  between operations  0.88 us (1%)
    pallas_call x1, Pallas kernels, experts(): pl.pallas_call(functools.partial(expert_kernel, n, cap), out_shape=jax.Sh...  37 us
    pallas_call x1, Pallas kernels, project(): pl.pallas_call(functools.partial(project_kernel, n), out_shape=(jax.Shape...  23.3 us
    pallas_call x1, Pallas kernels, state_update(): pl.pallas_call(state_kernel, grid=(rows,), out_shape=(jax.ShapeDtypeStruc...  8.03 us
    unnamed x23, local copies, waits for them, and re-layouts  4.51 us
    slice x2, local copies, waits for them, and re-layouts, body(): fresh = jnp.concatenate([x8[:rows], bc8[:rows]], axis=1).astype(BF16)  1.7 us

commit v1 on v0

v1 whole, which is shorter than its diff:
```python
import functools

import jax
import jax.numpy as jnp
from jax import lax
from jax.experimental import pallas as pl
from jax.experimental.pallas import tpu as pltpu
from jax.sharding import PartitionSpec as P

HEADS = 64
HEAD_DIM = 64
SSM_GROUPS = 4
STATE = 64
TOP = 4
EPS = 1e-06
MESH = pl.DeviceIdType.MESH
F32 = jnp.float32
BF16 = jnp.bfloat16
ROWS = 8
INNER = HEADS * HEAD_DIM
SPAN = SSM_GROUPS * STATE


def rms_scale(values, gain_vec):
    return (
        values
        * lax.rsqrt(jnp.mean(values * values, axis=-1, keepdims=True) + EPS)
        * gain_vec.astype(F32)
    )


def dot(a, b):
    return jnp.dot(a, b, preferred_element_type=F32)


def dot_nt(a, b):
    return lax.dot_general(a, b, (((1,), (1,)), ((), ())), preferred_element_type=F32)


def iota(shape, axis):
    return lax.broadcasted_iota(jnp.int32, shape, axis)


def onehot(mask):
    return mask.astype(F32).astype(BF16)


def peer(index):
    return (lax.axis_index("grp"), index)


def remote(src, dst, send_sem, recv_sem, index):
    return pltpu.make_async_remote_copy(
        src_ref=src,
        dst_ref=dst,
        send_sem=send_sem,
        recv_sem=recv_sem,
        device_id=peer(index),
        device_id_type=MESH,
    )


def spread(ref):
    value = ref[...].astype(F32)
    return jnp.concatenate([value[i : i + 1] for i in range(value.shape[0])], axis=1)


def column(row):
    size = row.shape[1]
    at = iota((size, size), 0)
    to = iota((size, size), 1)
    return jnp.sum(jnp.where(at == to, row, jnp.zeros_like(row)), axis=1, keepdims=True)


class Gather:
    def __init__(self, n, buf, send, recv):
        self.n, self.buf, self.send, self.recv = n, buf, send, recv
        self.me = lax.axis_index("ep")
        self.outer = n // 4
        core = lax.rem(self.me, 2)
        mid = lax.rem(self.me // 2, 2)
        self.mate = self.me + 1 - 2 * core
        self.across = self.me + 2 - 4 * mid

    def go(self, src, block, kind, d, to):
        sem = self.recv.at[kind * self.outer + d]
        remote(src, self.buf.at[block], self.send.at[0], sem, to).start()

    def arrive(self, block, kind, d):
        sem = self.recv.at[kind * self.outer + d]
        piece = self.buf.at[block]
        remote(piece, piece, self.send.at[0], sem, self.mate).wait_recv()

    def start(self, src):
        for d in range(1, self.outer):
            self.go(src, self.me, 0, d, lax.rem(self.me + 4 * d, self.n))
        self.go(src, self.me, 1, 0, self.across)
        self.go(src, self.me, 2, 0, self.mate)

    def near(self, d):
        return lax.rem(self.me + self.n - 4 * d, self.n)

    def far(self, d):
        return lax.rem(self.across + self.n - 4 * d, self.n)

    def middle(self):
        for d in range(1, self.outer):
            block = self.near(d)
            self.arrive(block, 0, d)
            self.go(self.buf.at[block], block, 1, d, self.across)
            self.go(self.buf.at[block], block, 2, d, self.mate)

    def last(self):
        for d in range(self.outer):
            block = self.far(d)
            self.arrive(block, 1, d)
            self.go(self.buf.at[block], block, 3, d, self.mate)

    def finish(self):
        for kind in (2, 3):
            for d in range(self.outer):
                self.arrive(self.me, kind, d)

    def drain(self):
        piece = self.buf.at[pl.ds(0, self.n - 1)]
        remote(piece, piece, self.send.at[0], self.recv.at[0], self.mate).wait_send()


class Exchange:
    def __init__(self, n, out_buf, in_buf, send, recv):
        self.n, self.out_buf, self.in_buf, self.send, self.recv = n, out_buf, in_buf, send, recv
        self.me = lax.axis_index("ep")

    def start(self):
        for d in range(1, self.n):
            to = lax.rem(self.me + d, self.n)
            remote(
                self.out_buf.at[to], self.in_buf.at[self.me], self.send.at[0], self.recv.at[0], to
            ).start()
        self.in_buf[self.me] = self.out_buf[self.me]

    def _all(self):
        part = pl.ds(0, self.n - 1)
        return remote(
            self.out_buf.at[part], self.in_buf.at[part], self.send.at[0], self.recv.at[0], self.me
        )

    def wait(self):
        self._all().wait_recv()

    def drain(self):
        self._all().wait_send()


def mixer_kernel(n, cap, *refs):
    (
        own_ref,
        ids_ref,
        prob_ref,
        score_ref,
        conv_ref,
        taps_ref,
        bias_ref,
        g1_ref,
        gi_ref,
        g2_ref,
        dtb_ref,
        dlog_ref,
        skip_ref,
        z_any,
        x_any,
        b_any,
        c_any,
        dt_any,
        ow_any,
        eg_any,
        eu_any,
        ed_any,
        st_any,
        out_ref,
        sx_ref,
        decx_ref,
        bc_ref,
        fresh_ref,
        hid,
        hbuf,
        hall,
        hg,
        hsq,
        zw,
        xw,
        bw,
        cw,
        dw,
        ow,
        eg,
        eu,
        ed,
        st,
        prod,
        fold,
        r0s,
        stepx,
        cpart,
        pre_out,
        pre_in,
        x_out,
        x_in,
        yown,
        ybuf,
        sel,
        bigh,
        bigl,
        hsel,
        p_out,
        p_in,
        mg,
        stage,
        spot_rows,
        o_out,
        o_in,
        wsem,
        gs,
        gr,
        as_,
        ar,
    ) = refs
    rows, width = own_ref.shape
    cols = zw.shape[1]
    ncol = ow.shape[1]
    total = n * ROWS
    slots = n * cap
    sp = sel.shape[0] // n
    chunks = width // 128
    per = HEADS // SSM_GROUPS
    me = lax.axis_index("ep")

    pairs = [(b_any, bw), (c_any, cw), (dt_any, dw)]
    pairs += [(st_any.at[t], st.at[t]) for t in range(rows)]
    pairs += [(x_any, xw), (z_any, zw), (ow_any, ow)]
    pairs += [(eg_any.at[0], eg), (eu_any.at[0], eu), (ed_any.at[0], ed)]
    loads = [pltpu.make_async_copy(src, dst, wsem.at[i]) for i, (src, dst) in enumerate(pairs)]
    for load in loads:
        load.start()

    barrier = pltpu.get_barrier_semaphore()
    for d in range(1, n):
        pl.semaphore_signal(
            barrier, inc=1, device_id=peer(lax.rem(me + d, n)), device_id_type=MESH
        )
    ids = ids_ref[...].astype(F32)
    pick = iota((TOP, 128), 0)
    lane = iota((TOP, 128), 1)
    spot = jnp.zeros((TOP, 128), F32)
    for r in range(rows):
        spot = spot + jnp.where(lane == TOP * r + pick, ids[:, r : r + 1] + 1.0, 0.0)
    id_row = jnp.sum(spot, axis=0, keepdims=True) - 1.0
    id_row = jnp.concatenate([id_row, jnp.full((1, width - 128), -1.0, F32)], axis=1)
    hid[...] = jnp.concatenate([own_ref[...].astype(F32), id_row], axis=0).astype(BF16)
    pl.semaphore_wait(barrier, n - 1)

    hidden_ag = Gather(n, hbuf, gs.at[pl.ds(0, 1)], gr.at[pl.ds(0, n)])
    hidden_ag.start(hid)
    hbuf[me] = hid[...]

    gain1 = spread(g1_ref)
    own = hid[...].astype(F32)
    mine = rms_scale(own, gain1).astype(BF16)
    taps = taps_ref[...].astype(F32)
    held = conv_ref.shape[0]
    summed = spread(bias_ref)
    for k in range(held):
        summed = summed + conv_ref[k].astype(F32) * taps[k : k + 1]
    cpart[...] = jnp.concatenate([summed, jnp.zeros((ROWS - rows, summed.shape[1]), F32)], axis=0)
    for load in loads[:3]:
        load.wait()
    fresh_b = dot(mine, bw[...]).astype(BF16)
    fresh_c = dot(mine, cw[...]).astype(BF16)
    fresh_ref[:, INNER : INNER + SPAN] = fresh_b
    fresh_ref[:, INNER + SPAN :] = fresh_c
    b_act = jax.nn.silu(
        cpart[:, INNER : INNER + SPAN]
        + fresh_b.astype(F32) * taps[held : held + 1, INNER : INNER + SPAN]
    )
    c_act = jax.nn.silu(
        cpart[:, INNER + SPAN :] + fresh_c.astype(F32) * taps[held : held + 1, INNER + SPAN :]
    )
    bc_ref[:, :SPAN] = b_act
    bc_ref[:, SPAN:] = c_act
    dt = dot_nt(mine, dw[...]).astype(BF16).astype(F32)
    step = jax.nn.softplus(dt + dtb_ref[...])
    dt_t = dot_nt(dw[...], mine).astype(BF16).astype(F32)
    step_t = jax.nn.softplus(dt_t + column(dtb_ref[...]))
    decay_t = jnp.exp(-step_t * jnp.exp(column(dlog_ref[...])))
    for t in range(rows):
        at = slice(t * HEADS, (t + 1) * HEADS)
        stepx[at, :] = jnp.broadcast_to(step_t[:, t : t + 1], (HEADS, 128))
        decx_ref[at, :] = jnp.broadcast_to(decay_t[:, t : t + 1], (HEADS, 128))
    pad = slice(rows * HEADS, ROWS * HEADS)
    stepx[pad, :] = jnp.zeros(((ROWS - rows) * HEADS, 128), F32)
    decx_ref[pad, :] = jnp.zeros(((ROWS - rows) * HEADS, 128), F32)
    r0s[pad, :] = jnp.zeros(((ROWS - rows) * HEADS, 128), F32)
    bc = b_act * c_act
    bc_hi = bc.astype(BF16)
    bc_lo = (bc - bc_hi.astype(F32)).astype(BF16)
    group = onehot(iota((SPAN, 128), 0) // STATE == iota((SPAN, 128), 1) // per)
    inner = dot(bc_hi, group) + dot(bc_lo, group)
    coef = step * inner[:, :HEADS] + skip_ref[...]
    row_ok = iota((ROWS, HEADS), 0) < rows
    coef = jnp.where(row_ok, coef, 0.0)
    coef = jnp.concatenate([coef, jnp.zeros((ROWS, 128 - HEADS), F32)], axis=1).astype(BF16)

    hidden_ag.middle()

    def make_fold(i, carry):
        at = pl.ds(pl.multiple_of(i * 256, 256), 256)
        p_of = iota((256, 128), 0) // STATE + 4 * i
        fold[at, :] = onehot(p_of == lax.rem(iota((256, 128), 1), HEAD_DIM))
        return carry

    lax.fori_loop(0, INNER // 256, make_fold, 0)

    def make_prod(t, carry):
        pltpu.make_async_copy(st_any.at[t], st.at[t], wsem.at[3 + t]).wait()
        row = bc_ref[pl.ds(t, 1), :]
        cs = []
        for g in range(SSM_GROUPS):
            c = row[:, SPAN + g * STATE : SPAN + (g + 1) * STATE]
            cs.append(jnp.broadcast_to(jnp.concatenate([c, c], axis=1), (per, 2 * STATE)))
        c_all = jnp.concatenate(cs, axis=0)
        at = pl.ds(pl.multiple_of(t * HEADS, HEADS), HEADS)
        for k in range(HEAD_DIM * STATE // 128):
            lanes = slice(k * 128, (k + 1) * 128)
            prod[at, lanes] = (st[t, :, lanes] * c_all).astype(BF16)
        return carry

    lax.fori_loop(0, rows, make_prod, 0)
    r0 = dot(prod[...], fold[...])
    r0s[: rows * HEADS, :] = r0 * decx_ref[: rows * HEADS, :]
    low_half = iota((ROWS, 128), 1) < HEAD_DIM
    for m in range(INNER // 128):
        even = r0s[pl.ds(2 * m, ROWS, stride=HEADS), :]
        odd = r0s[pl.ds(2 * m + 1, ROWS, stride=HEADS), :]
        j, off = (m * 128) // cols, (m * 128) % cols
        pre_out[j, :, off : off + 128] = jnp.where(low_half, even, odd).astype(BF16)
    for j in range(n):
        pre_out[j, :, cols : 2 * cols] = cpart[:, j * cols : (j + 1) * cols].astype(BF16)
        pre_out[j, :, 2 * cols :] = coef
    pre = Exchange(n, pre_out, pre_in, as_.at[pl.ds(0, 1)], ar.at[pl.ds(0, 1)])
    pre.start()

    hidden_ag.last()
    hidden_ag.finish()
    for j in range(0, n, 2):
        at = slice(j * ROWS, (j + 2) * ROWS)
        pair = jnp.concatenate([hbuf[j].astype(F32), hbuf[j + 1].astype(F32)], axis=0)
        hall[at, :] = pair.astype(BF16)
        hg[at, :] = (pair * gain1).astype(BF16)
        hsq[at, :] = (pair * pair).astype(BF16)
    for load in loads[3 + rows : 5 + rows]:
        load.wait()
    ones = jnp.ones((width, 128), BF16)
    scale = lax.rsqrt(dot(hsq[...], ones) * (1.0 / width) + EPS)
    scale = jnp.concatenate([scale] * (cols // 128), axis=1)
    xp = (dot(hg[...], xw[...]) * scale).astype(BF16).astype(F32)
    zp = (dot(hg[...], zw[...]) * scale).astype(BF16).astype(F32)
    for j in range(n):
        x_out[j] = xp[j * ROWS : (j + 1) * ROWS].astype(BF16)
    my_cols = pl.ds(pl.multiple_of(me * cols, 128), cols)
    tap = taps_ref[:, my_cols].astype(F32)[held : held + 1]
    gain_all = spread(gi_ref)
    cpart_gain = jnp.broadcast_to(gain_all, (ROWS, INNER))
    stage[pl.ds(0, ROWS), :] = cpart_gain[:, :width]
    stage[pl.ds(ROWS, ROWS), :] = cpart_gain[:, width:]
    half_n = n // 2
    upper = me // half_n
    gain_cols = stage[
        pl.ds(pl.multiple_of(upper * ROWS, ROWS), ROWS),
        pl.ds(pl.multiple_of(lax.rem(me, half_n) * cols, 128), cols),
    ]
    pre.wait()
    for j in range(0, n, 2):
        ys = []
        for i in (j, j + 1):
            at = slice(i * ROWS, (i + 1) * ROWS)
            block = pre_in[i].astype(F32)
            xa = jax.nn.silu(block[:, cols : 2 * cols] + xp[at] * tap)
            packed = block[:, 2 * cols :]
            grown = []
            for k in range(cols // 128):
                index = (me * cols + k * 128) // HEAD_DIM + iota((ROWS, 128), 1) // HEAD_DIM
                grown.append(jnp.take_along_axis(packed, index, axis=1))
            readout = block[:, :cols] + jnp.concatenate(grown, axis=1) * xa
            ys.append(readout * jax.nn.silu(zp[at]) * gain_cols)
        yown[j * ROWS : (j + 2) * ROWS, :] = jnp.concatenate(ys, axis=0).astype(BF16)

    y_ag = Gather(n, ybuf, gs.at[pl.ds(1, 1)], gr.at[pl.ds(n, n)])
    y_ag.start(yown)
    back = Exchange(n, x_out, x_in, as_.at[pl.ds(1, 1)], ar.at[pl.ds(1, 1)])
    back.start()
    ybuf[me] = yown[...]

    q = iota((slots, total), 0)
    t_of = iota((slots, total), 1)
    last = onehot(t_of == lax.rem(q, n) * ROWS + (ROWS - 1))
    id_all = dot(last, hall[:, :128])
    f_lane = iota((128, total), 0) // TOP
    token = lax.rem(iota((128, total), 1), ROWS)
    m_here = onehot(f_lane == token)
    m_less = onehot(f_lane < token)
    flags = jnp.concatenate([onehot(id_all == float(e)) for e in range(n)], axis=0)
    here = dot(flags, m_here)
    before = dot(flags, m_less)
    same = lax.rem(q, n) == t_of // ROWS
    rank_q = (q // n).astype(F32)
    own_row = iota((ROWS, total), 0)
    own_col = iota((ROWS, total), 1)
    for e in range(n):
        at = slice(e * slots, (e + 1) * slots)
        chosen = same & (here[at] > 0.5) & (before[at] == rank_q)
        tail = [(own_col == e * ROWS + own_row).astype(F32)]
        if sp > slots + ROWS:
            tail.append(jnp.zeros((sp - slots - ROWS, total), F32))
        sel[e * sp : (e + 1) * sp, :] = jnp.concatenate(
            [chosen.astype(F32)] + tail, axis=0
        ).astype(BF16)

    y_ag.middle()

    span = chunks * cap
    wide = n * span
    col = iota((rows, wide), 1).astype(F32)
    e_of = jnp.floor((col + 0.5) * (1.0 / span))
    in_e = col - e_of * span
    k_of = jnp.floor((in_e + 0.5) * (1.0 / cap))
    r_of = in_e - k_of * cap
    score = score_ref[...]
    share = prob_ref[...] * score / jnp.sum(score, axis=0, keepdims=True)
    weight = jnp.zeros((rows, wide), F32)
    used = jnp.zeros((rows, wide), F32)
    for i in range(TOP):
        hit = (column(ids[i : i + 1]) == e_of).astype(F32)
        used = used + hit
        weight = weight + hit * column(share[i : i + 1])
    row_id = iota((rows, wide), 0)
    rank = jnp.zeros((rows, wide), F32)
    for r in range(rows - 1):
        rank = rank + jnp.where(row_id > r, used[r : r + 1, :], 0.0)
    weight = jnp.where(rank == r_of, weight, 0.0)
    weight = jnp.concatenate([weight, jnp.zeros((ROWS - rows, wide), F32)], axis=0)
    k_row = k_of[0:1]
    for k in range(0, chunks, 2):
        both = jnp.concatenate(
            [jnp.where(k_row == float(k + i), weight, 0.0) for i in range(2)], axis=0
        )
        high = both.astype(BF16)
        at = slice(k * ROWS, (k + 2) * ROWS)
        bigh[at, :] = high
        bigl[at, :] = (both - high.astype(F32)).astype(BF16)
    pick_me = sel[pl.ds(pl.multiple_of(me * sp, 16), sp), :][:slots]
    hsel[...] = dot(pick_me, hall[...])

    y_ag.last()

    back.wait()
    for j in range(n):
        xv = x_in[j]
        fresh_ref[:, j * cols : (j + 1) * cols] = xv
        at = slice(j * cols, (j + 1) * cols)
        xa = jax.nn.silu(cpart[:, at] + xv.astype(F32) * taps_ref[held : held + 1, at].astype(F32))
        for k in range(cols // 128):
            m = (j * cols) // 128 + k
            piece = xa[:, k * 128 : (k + 1) * 128]
            sx_ref[pl.ds(2 * m, ROWS, stride=HEADS), :] = piece
            sx_ref[pl.ds(2 * m + 1, ROWS, stride=HEADS), :] = pltpu.roll(piece, HEAD_DIM, 1)
    sx_ref[...] = sx_ref[...] * stepx[...]

    loads[5 + rows].wait()
    y_ag.finish()
    acc = jnp.zeros((total, ncol), F32)
    ssq = jnp.zeros((total, 128), F32)
    inv_gain = (1.0 / gain_all).astype(BF16)
    ones_c = jnp.ones((cols, 128), BF16)
    for j in range(n):
        at = slice(j * cols, (j + 1) * cols)
        yb = ybuf[j]
        acc = acc + dot(yb, ow[at, :])
        raw = yb * inv_gain[:, at]
        ssq = ssq + dot(raw * raw, ones_c)
    scale = lax.rsqrt(ssq * (1.0 / INNER) + EPS)
    p = (acc * scale[:, :ncol]).astype(BF16)
    picked = dot(sel[...], p).astype(BF16)
    for e in range(n):
        p_out[e] = picked[e * sp : e * sp + slots + ROWS]
    p_ex = Exchange(n, p_out, p_in, as_.at[pl.ds(2, 1)], ar.at[pl.ds(2, 1)])
    p_ex.start()
    gain2 = spread(g2_ref)
    for load in loads[6 + rows :]:
        load.wait()
    p_ex.wait()
    ssq = jnp.zeros((slots, 128), F32)
    ones_n = jnp.ones((ncol, 128), BF16)
    mixed = []
    for j in range(n):
        at = slice(j * ncol, (j + 1) * ncol)
        block = p_in[j].astype(F32)
        m = (hsel[:, at] + block[:slots]).astype(BF16).astype(F32)
        mg[:, at] = (m * gain2[:, at]).astype(BF16)
        ssq = ssq + dot((m * m).astype(BF16), ones_n)
        mixed.append((own[:, at] + block[slots:]).astype(BF16).astype(F32))
    mixed = jnp.concatenate(mixed, axis=1)
    scale = lax.rsqrt(ssq * (1.0 / width) + EPS)
    acts = []
    for j in range(0, eg.shape[1], 128):
        at = slice(j, j + 128)
        gate = dot(mg[...], eg[:, at]) * scale
        up = dot(mg[...], eu[:, at]) * scale
        acts.append((jax.nn.silu(gate) * up).astype(BF16))
    act = jnp.concatenate(acts, axis=1)
    for k in range(0, chunks, 2):
        part = dot(act, ed[:, k * 128 : (k + 2) * 128])
        for i in range(2):
            for r in range(cap):
                spot_rows[pl.ds((k + i) * cap + r, n, stride=span), :] = part[
                    r * n : (r + 1) * n, i * 128 : (i + 1) * 128
                ]
    for s in range(n):
        o_out[s] = spot_rows[s * span : (s + 1) * span, :].astype(BF16)
    o_ex = Exchange(n, o_out, o_in, as_.at[pl.ds(3, 1)], ar.at[pl.ds(3, 1)])
    o_ex.start()
    hidden_ag.drain()
    y_ag.drain()
    pre.drain()
    back.drain()
    p_ex.drain()
    o_ex.wait()
    got = jnp.concatenate([o_in[e] for e in range(n)], axis=0)
    moe = dot(bigh[...], got) + dot(bigl[...], got)
    for k in range(chunks):
        at = slice(k * 128, (k + 1) * 128)
        out_ref[:, at] = (mixed[:, at] + moe[k * ROWS : (k + 1) * ROWS])[:rows].astype(BF16)
    o_ex.drain()


def mixer(n, cap, args, rows, width, z_weight, out_weight, expert_gate, expert_down):
    cols = z_weight.shape[1]
    ncol = out_weight.shape[1]
    units = expert_gate.shape[2]
    total = n * ROWS
    slots = n * cap
    sp = (slots + ROWS + 15) // 16 * 16
    chunks = width // 128
    span = chunks * cap
    vm = pl.BlockSpec(memory_space=pltpu.VMEM)
    hbm = pl.BlockSpec(memory_space=pl.ANY)
    dma = pltpu.SemaphoreType.DMA

    def buf(*shape, dtype=BF16):
        return pltpu.VMEM(shape, dtype)

    return pl.pallas_call(
        functools.partial(mixer_kernel, n, cap),
        out_shape=(
            jax.ShapeDtypeStruct((rows, width), BF16),
            jax.ShapeDtypeStruct((ROWS * HEADS, 128), F32),
            jax.ShapeDtypeStruct((ROWS * HEADS, 128), F32),
            jax.ShapeDtypeStruct((ROWS, 2 * SPAN), F32),
            jax.ShapeDtypeStruct((ROWS, INNER + 2 * SPAN), BF16),
        ),
        in_specs=[vm] * 13 + [hbm] * 10,
        out_specs=(vm,) * 5,
        scratch_shapes=[
            buf(ROWS, width),
            buf(n, ROWS, width),
            buf(total, width),
            buf(total, width),
            buf(total, width),
            buf(width, cols),
            buf(width, cols),
            buf(width, SPAN),
            buf(width, SPAN),
            buf(HEADS, width),
            buf(INNER, ncol),
            buf(width, units),
            buf(width, units),
            buf(units, width),
            buf(rows, HEADS, HEAD_DIM * STATE, dtype=F32),
            buf(rows * HEADS, HEAD_DIM * STATE),
            buf(INNER, 128),
            buf(ROWS * HEADS, 128, dtype=F32),
            buf(ROWS * HEADS, 128, dtype=F32),
            buf(ROWS, INNER + 2 * SPAN, dtype=F32),
            buf(n, ROWS, 2 * cols + 128),
            buf(n, ROWS, 2 * cols + 128),
            buf(n, ROWS, cols),
            buf(n, ROWS, cols),
            buf(total, cols),
            buf(n, total, cols),
            buf(n * sp, total),
            buf(chunks * ROWS, n * span),
            buf(chunks * ROWS, n * span),
            buf(slots, width, dtype=F32),
            buf(n, slots + ROWS, ncol),
            buf(n, slots + ROWS, ncol),
            buf(slots, width),
            buf(2 * ROWS, width, dtype=F32),
            buf(n * span, 128, dtype=F32),
            buf(n, span, 128),
            buf(n, span, 128),
            dma((9 + rows,)),
            dma((2,)),
            dma((2 * n,)),
            dma((4,)),
            dma((4,)),
        ],
        compiler_params=pltpu.CompilerParams(
            collective_id=0, has_side_effects=True, vmem_limit_bytes=56 << 20
        ),
        name="mixer",
    )(*args)


def state_kernel(
    sx_ref, dec_ref, bc_ref, fresh_ref, conv_ref, layer_ref, st_ref, out_ref, conv_out, lay, e_ref
):
    s = pl.program_id(0)
    rows = layer_ref.shape[0]
    blocks = HEAD_DIM * STATE // 256

    @pl.when(s == 0)
    def _():
        held = conv_ref.shape[0]
        for k in range(1, held):
            conv_out[k - 1] = conv_ref[k]
        conv_out[held - 1] = fresh_ref[...][:rows]
        lay[...] = layer_ref[...]

        def make(k, carry):
            at = pl.ds(pl.multiple_of(k * 256, 256), 256)
            p_of = iota((128, 256), 1) // STATE + 4 * k
            e_ref[:, at] = onehot(p_of == lax.rem(iota((128, 256), 0), HEAD_DIM))
            return carry

        lax.fori_loop(0, blocks, make, 0)

    sx = sx_ref[...]
    high = sx.astype(BF16).astype(F32)
    low = pltpu.roll(sx - high, HEAD_DIM, 1)
    lhs = jnp.where(iota((HEADS, 128), 1) < HEAD_DIM, high, low).astype(BF16)
    dec = dec_ref[...]
    row = bc_ref[pl.ds(s, 1), :]
    per = HEADS // SSM_GROUPS
    bs = []
    for g in range(SSM_GROUPS):
        b = row[:, g * STATE : (g + 1) * STATE]
        bs.append(jnp.broadcast_to(jnp.concatenate([b, b], axis=1), (per, 2 * STATE)))
    b_all = jnp.concatenate(bs, axis=0)
    for k in range(blocks):
        grown = dot(lhs, e_ref[:, k * 256 : (k + 1) * 256])
        for i in range(2):
            at = slice((2 * k + i) * 128, (2 * k + i + 1) * 128)
            out_ref[0, :, at] = dec * st_ref[0, :, at] + grown[:, i * 128 : (i + 1) * 128] * b_all


def state_update(sx, dec, bc, fresh, conv_t, layer, state_in):
    rows, _, flat = state_in.shape

    def whole(x):
        return pl.BlockSpec(x.shape, lambda s: (0,) * len(x.shape))

    part = pl.BlockSpec((HEADS, 128), lambda s: (s, 0))
    block = pl.BlockSpec((1, HEADS, flat), lambda s: (s, 0, 0))
    return pl.pallas_call(
        state_kernel,
        grid=(rows,),
        out_shape=(
            jax.ShapeDtypeStruct(state_in.shape, F32),
            jax.ShapeDtypeStruct(conv_t.shape, BF16),
            jax.ShapeDtypeStruct(layer.shape, BF16),
        ),
        in_specs=[part, part, whole(bc), whole(fresh), whole(conv_t), whole(layer), block],
        out_specs=(block, whole(conv_t), whole(layer)),
        scratch_shapes=[pltpu.VMEM((128, flat), BF16)],
        compiler_params=pltpu.CompilerParams(vmem_limit_bytes=24 << 20),
        name="state",
    )(sx, dec, bc, fresh, conv_t, layer, state_in)


def body(
    hidden,
    state_in,
    conv_state,
    expert_ids,
    group_prob,
    expert_score,
    first_gain,
    z_weight,
    x_weight,
    b_weight,
    c_weight,
    dt_weight,
    conv_weight,
    conv_bias,
    dt_bias,
    decay_log,
    skip_gain,
    inner_gain,
    out_weight,
    second_gain,
    expert_gate,
    expert_up,
    expert_down,
):
    n = lax.axis_size("ep")
    rows, width = hidden.shape
    cap = max(2, (3 * rows * TOP + 2 * n - 1) // (2 * n))
    conv_t = conv_state.transpose(1, 0, 2)
    args = (
        hidden,
        expert_ids.T,
        group_prob[None, :],
        expert_score.T,
        conv_t,
        conv_weight,
        conv_bias.reshape(-1, 128),
        first_gain.reshape(-1, 128),
        inner_gain.reshape(-1, 128),
        second_gain.reshape(-1, 128),
        dt_bias[None, :],
        decay_log[None, :],
        skip_gain[None, :],
        z_weight,
        x_weight,
        b_weight,
        c_weight,
        dt_weight.T,
        out_weight,
        expert_gate,
        expert_up,
        expert_down,
        state_in,
    )
    layer, sx, dec, bc, fresh = mixer(
        n, cap, args, rows, width, z_weight, out_weight, expert_gate, expert_down
    )
    state_out, conv_out, layer_out = state_update(sx, dec, bc, fresh, conv_t, layer, state_in)
    return (layer_out, state_out, conv_out.transpose(1, 0, 2))


def solution(mesh):
    in_specs = (
        P(("grp", "ep"), None),
        P(("grp", "ep"), None, None),
        P(("grp", "ep"), None, None),
        P(("grp", "ep"), None),
        P(("grp", "ep")),
        P(("grp", "ep"), None),
        P(),
        P(None, "ep"),
        P(None, "ep"),
        P(),
        P(),
        P(),
        P(),
        P(),
        P(),
        P(),
        P(),
        P(),
        P(None, "ep"),
        P(),
        P("ep", None, None),
        P("ep", None, None),
        P("ep", None, None),
    )
    out_specs = (P(("grp", "ep"), None), P(("grp", "ep"), None, None), P(("grp", "ep"), None, None))
    return jax.shard_map(body, mesh=mesh, in_specs=in_specs, out_specs=out_specs, check_vma=False)
```

time: 78.9 us -> 61.1 us (0.77)
  Pallas kernels: 68.3 us -> 55.8 us
  local copies, waits for them, and re-layouts: 8.27 us -> 4.26 us
  other arithmetic: 1.09 us -> 0.01 us
    pallas_call x2 -> x1, Pallas kernels: 60.3 us -> 50.1 us  [mixer(): pl.pallas_call(functools.partial(mixer_kernel, n, cap), out_shape=(jax.Sh...]
    pallas_call x1, Pallas kernels: 8.03 us -> 5.67 us  [state_update(): pl.pallas_call(state_kernel, grid=(rows,), out_shape=(jax.ShapeDtypeStruc...]
    slice x8 -> x0, local copies, waits for them, and re-layouts: 1.78 us -> none  [the longest x2 1.7 us: body(): fresh = jnp.concatenate([x8[:rows], bc8[:rows]], axis=1).astype(BF16)]
    concatenate x2 -> x0, other arithmetic: 0.91 us -> none  [the longest x1 0.72 us: body(): conv_out = jnp.concatenate([conv_state[:, 1:], fresh[:, None, :]], axis=1)]
    broadcast_in_dim x2 -> x0, local copies, waits for them, and re-layouts: 0.81 us -> none  [body(): dt8[:rows][:, :, None]]
    unnamed x23 -> x16, local copies, waits for them, and re-layouts: 4.51 us -> 4.26 us
where the time goes in v1:
time: 61.1 us; the launch traced here: 60.7 us
  Pallas kernels  55.8 us (91%)
  local copies, waits for them, and re-layouts  4.26 us (7%)
  between operations  0.71 us (1%)
    pallas_call x1, Pallas kernels, mixer(): pl.pallas_call(functools.partial(mixer_kernel, n, cap), out_shape=(jax.Sh...  50.1 us
    pallas_call x1, Pallas kernels, state_update(): pl.pallas_call(state_kernel, grid=(rows,), out_shape=(jax.ShapeDtypeStruc...  5.67 us
    unnamed x16, local copies, waits for them, and re-layouts  4.26 us

profile of v1, /device:TPU:0, one launch (start us, length us, event | category | flops | bytes accessed | tf_op | source)
XLA Modules:
  0.0 60.7 jit_solution(11199027014760468648)
XLA Ops:
  0.6 0.0 slice-start
  0.6 0.0 slice-start.1
  0.7 0.0 copy-start
  0.7 50.1 %mixer.1 = (bf16[7,2048]{1,0:T(8,128)(2,1)}, f32[512,128]{1,0:T(8,128)}, f32[512,128]{1,0:T(8,128)}, f32[8,512]{1,0:T(8,128)}, bf16[8,4608]{1,0:T(8,128)(2,1)}) custom-call(bf16[7,2048]{1,0:T(8,128)(2,1)} %refs_0_.1, s32[4,7]{1,0:T(4,128)} %bitcast.22, f32[1,7]{1,0:T(1,128)} %bitcast.24, f32[4,7]{1,0:T(4,128)} %bitcast.23, bf16[3,7,4608]{2,1,0:T(8,128)(2,1)} %bitcast.15, ...), custom_call_target="tpu_custom_call" | custom-call | tf_op jit(solution)/shard_map/mixer/pallas_call | solution.py:561
  50.8 0.0 slice-done
  50.8 0.0 slice-done.1
  50.8 0.0 copy-done
  50.8 0.0 copy-start.1
  50.8 0.9 %copy-done.1 = f32[512,128]{1,0:T(8,128)S(1)} copy-done((f32[512,128]{1,0:T(8,128)S(1)}, f32[512,128]{1,0:T(8,128)}, u32[]{:S(2)}) %copy-start.1) | copy-done | bytes 262168
  51.7 0.0 copy-start.2
  51.7 0.9 %copy-done.2 = f32[512,128]{1,0:T(8,128)S(1)} copy-done((f32[512,128]{1,0:T(8,128)S(1)}, f32[512,128]{1,0:T(8,128)}, u32[]{:S(2)}) %copy-start.2) | copy-done | bytes 262168
  52.7 0.0 copy-start.3
  52.7 0.9 %copy-done.3 = bf16[8,4608]{1,0:T(8,128)(2,1)S(1)} copy-done((bf16[8,4608]{1,0:T(8,128)(2,1)S(1)}, bf16[8,4608]{1,0:T(8,128)(2,1)}, u32[]{:S(2)}) %copy-start.3) | copy-done | bytes 73752
  53.6 0.0 copy-start.4
  53.6 0.8 %copy-done.4 = bf16[7,2048]{1,0:T(8,128)(2,1)S(1)} copy-done((bf16[7,2048]{1,0:T(8,128)(2,1)S(1)}, bf16[7,2048]{1,0:T(8,128)(2,1)}, u32[]{:S(2)}) %copy-start.4) | copy-done | bytes 28696
  54.3 0.0 copy-start.5
  54.3 0.7 %copy-done.5 = f32[8,512]{1,0:T(8,128)S(1)} copy-done((f32[8,512]{1,0:T(8,128)S(1)}, f32[8,512]{1,0:T(8,128)}, u32[]{:S(2)}) %copy-start.5) | copy-done | bytes 16408
  55.1 5.7 %state.1 = (f32[7,64,4096]{2,1,0:T(8,128)}, bf16[3,7,4608]{2,1,0:T(8,128)(2,1)}, bf16[7,2048]{1,0:T(8,128)(2,1)}) custom-call(f32[512,128]{1,0:T(8,128)S(1)} %copy-done.1, f32[512,128]{1,0:T(8,128)S(1)} %copy-done.2, f32[8,512]{1,0:T(8,128)S(1)} %copy-done.5, bf16[8,4608]{1,0:T(8,128)(2,1)S(1)} %copy-done.3, bf16[3,7,4608]{2,1,0:T(8,128)(2,1)S(1)} %bitcast.16, ...), custom_call_target="tpu_custom_call" | custom-call | tf_op jit(solution)/shard_map/state/pallas_call | solution.py:673
  (1 shorter events, 0.0 us)
Async XLA Ops:
  0.6 50.1 %slice-start = ((s8[7340032]{0:T(1024)(128)(4,1)}), s8[4194304]{0:T(1024)(128)(4,1)S(1)}, s32[]{:S(2)}) async-start(s8[7340032]{0:T(1024)(128)(4,1)} %bitcast.13), calls=%async_computation | async-start | bytes 8388608
  0.6 50.1 %slice-start.1 = ((s8[7340032]{0:T(1024)(128)(4,1)}), s8[3145728]{0:T(1024)(128)(4,1)S(1)}, s32[]{:S(2)}) async-start(s8[7340032]{0:T(1024)(128)(4,1)} %bitcast.13), calls=%async_computation.1 | async-start | bytes 6291456
  0.7 50.1 %copy-start = (bf16[7,3,4608]{2,0,1:T(8,128)(2,1)S(1)}, bf16[7,3,4608]{2,0,1:T(8,128)(2,1)}, u32[]{:S(2)}) copy-start(bf16[7,3,4608]{2,0,1:T(8,128)(2,1)} %param.25) | copy-start | bytes 580612
  50.8 1.0 %copy-start.1 = (f32[512,128]{1,0:T(8,128)S(1)}, f32[512,128]{1,0:T(8,128)}, u32[]{:S(2)}) copy-start(f32[512,128]{1,0:T(8,128)} %get-tuple-element.11.sx_ref) | copy-start | bytes 786436
  51.7 0.9 %copy-start.2 = (f32[512,128]{1,0:T(8,128)S(1)}, f32[512,128]{1,0:T(8,128)}, u32[]{:S(2)}) copy-start(f32[512,128]{1,0:T(8,128)} %get-tuple-element.12.dec_ref) | copy-start | bytes 786436
  52.7 0.9 %copy-start.3 = (bf16[8,4608]{1,0:T(8,128)(2,1)S(1)}, bf16[8,4608]{1,0:T(8,128)(2,1)}, u32[]{:S(2)}) copy-start(bf16[8,4608]{1,0:T(8,128)(2,1)} %get-tuple-element.14.fresh_ref) | copy-start | bytes 221188
  53.6 0.8 %copy-start.4 = (bf16[7,2048]{1,0:T(8,128)(2,1)S(1)}, bf16[7,2048]{1,0:T(8,128)(2,1)}, u32[]{:S(2)}) copy-start(bf16[7,2048]{1,0:T(8,128)(2,1)} %get-tuple-element.15.layer_ref) | copy-start | bytes 86020
  54.3 0.7 %copy-start.5 = (f32[8,512]{1,0:T(8,128)S(1)}, f32[8,512]{1,0:T(8,128)}, u32[]{:S(2)}) copy-start(f32[8,512]{1,0:T(8,128)} %get-tuple-element.13.bc_ref) | copy-start | bytes 49156

commit v2 on v1

--- a/solution.py
+++ b/solution.py
@@ -73,8 +73,10 @@
 
 
 class Gather:
-    def __init__(self, n, buf, send, recv):
+    def __init__(self, n, buf, send, recv, split=1, direct=False):
         self.n, self.buf, self.send, self.recv = n, buf, send, recv
+        self.split, self.direct = split, direct
+        self.size = buf.shape[1] // split
         self.me = lax.axis_index("ep")
         self.outer = n // 4
         core = lax.rem(self.me, 2)
@@ -82,20 +84,30 @@
         self.mate = self.me + 1 - 2 * core
         self.across = self.me + 2 - 4 * mid
 
-    def go(self, src, block, kind, d, to):
-        sem = self.recv.at[kind * self.outer + d]
-        remote(src, self.buf.at[block], self.send.at[0], sem, to).start()
-
-    def arrive(self, block, kind, d):
-        sem = self.recv.at[kind * self.outer + d]
-        piece = self.buf.at[block]
-        remote(piece, piece, self.send.at[0], sem, self.mate).wait_recv()
+    def at(self, k):
+        return pl.ds(k * self.size, self.size)
+
+    def sem(self, kind, d, k):
+        return self.recv.at[(kind * self.outer + d) * self.split + k]
+
+    def go(self, src, block, kind, d, k, to):
+        dst = self.buf.at[block, self.at(k)]
+        remote(src, dst, self.send.at[0], self.sem(kind, d, k), to).start()
+
+    def arrive(self, block, kind, d, k):
+        piece = self.buf.at[block, self.at(k)]
+        remote(piece, piece, self.send.at[0], self.sem(kind, d, k), self.mate).wait_recv()
 
     def start(self, src):
-        for d in range(1, self.outer):
-            self.go(src, self.me, 0, d, lax.rem(self.me + 4 * d, self.n))
-        self.go(src, self.me, 1, 0, self.across)
-        self.go(src, self.me, 2, 0, self.mate)
+        for k in range(self.split):
+            piece = src.at[self.at(k)]
+            for d in range(1, self.outer):
+                far = lax.rem(self.across + 4 * d, self.n)
+                if self.direct:
+                    self.go(piece, self.me, 1, d, k, far)
+                self.go(piece, self.me, 0, d, k, lax.rem(self.me + 4 * d, self.n))
+            self.go(piece, self.me, 1, 0, k, self.across)
+            self.go(piece, self.me, 2, 0, k, self.mate)
 
     def near(self, d):
         return lax.rem(self.me + self.n - 4 * d, self.n)
@@ -104,22 +116,26 @@
         return lax.rem(self.across + self.n - 4 * d, self.n)
 
     def middle(self):
-        for d in range(1, self.outer):
-            block = self.near(d)
-            self.arrive(block, 0, d)
-            self.go(self.buf.at[block], block, 1, d, self.across)
-            self.go(self.buf.at[block], block, 2, d, self.mate)
+        for k in range(self.split):
+            for d in range(1, self.outer):
+                block = self.near(d)
+                self.arrive(block, 0, d, k)
+                piece = self.buf.at[block, self.at(k)]
+                if not self.direct:
+                    self.go(piece, block, 1, d, k, self.across)
+                self.go(piece, block, 2, d, k, self.mate)
 
     def last(self):
-        for d in range(self.outer):
-            block = self.far(d)
-            self.arrive(block, 1, d)
-            self.go(self.buf.at[block], block, 3, d, self.mate)
-
-    def finish(self):
-        for kind in (2, 3):
+        for k in range(self.split):
             for d in range(self.outer):
-                self.arrive(self.me, kind, d)
+                block = self.far(d)
+                self.arrive(block, 1, d, k)
+                self.go(self.buf.at[block, self.at(k)], block, 3, d, k, self.mate)
+
+    def finish(self, kind):
+        for k in range(self.split):
+            for d in range(self.outer):
+                self.arrive(self.me, kind, d, k)
 
     def drain(self):
         piece = self.buf.at[pl.ds(0, self.n - 1)]
@@ -127,33 +143,76 @@
 
 
 class Exchange:
-    def __init__(self, n, out_buf, in_buf, send, recv):
+    def __init__(self, n, out_buf, in_buf, send, recv, planes=False):
         self.n, self.out_buf, self.in_buf, self.send, self.recv = n, out_buf, in_buf, send, recv
         self.me = lax.axis_index("ep")
+        self.z = self.me // 4
+        self.w = lax.rem(self.me, 4)
+        self.half = n // 8
+        self.a = self.z // self.half
+        self.b = lax.rem(self.z, self.half)
+        self.planes = planes
+
+    def order(self):
+        near = [self.a * self.half + lax.rem(self.b + i, self.half) for i in range(self.half)]
+        far = [(1 - self.a) * self.half + lax.rem(self.b + i, self.half) for i in range(self.half)]
+        return near + far
 
     def start(self):
-        for d in range(1, self.n):
-            to = lax.rem(self.me + d, self.n)
-            remote(
-                self.out_buf.at[to], self.in_buf.at[self.me], self.send.at[0], self.recv.at[0], to
-            ).start()
+        sem = self.recv.at[self.z] if self.planes else self.recv.at[0]
+        own, *near = self.order()
+        for plane in near[self.half - 1 :] + near[: self.half - 1] + [own]:
+            for i in range(4):
+                if plane is own and i == 0:
+                    continue
+                to = 4 * plane + lax.rem(self.w + i, 4)
+                remote(
+                    self.out_buf.at[to], self.in_buf.at[self.me], self.send.at[0], sem, to
+                ).start()
         self.in_buf[self.me] = self.out_buf[self.me]
 
-    def _all(self):
-        part = pl.ds(0, self.n - 1)
-        return remote(
-            self.out_buf.at[part], self.in_buf.at[part], self.send.at[0], self.recv.at[0], self.me
-        )
+    def _some(self, count, sem):
+        part = pl.ds(0, count)
+        return remote(self.out_buf.at[part], self.in_buf.at[part], self.send.at[0], sem, self.me)
 
     def wait(self):
-        self._all().wait_recv()
+        self._some(self.n - 1, self.recv.at[0]).wait_recv()
+
+    def wait_plane(self, index, plane):
+        self._some(3 if index == 0 else 4, self.recv.at[plane]).wait_recv()
 
     def drain(self):
-        self._all().wait_send()
+        self._some(self.n - 1, self.recv.at[0]).wait_send()
 
 
 def mixer_kernel(n, cap, *refs):
     (
+        own_any,
+        ids_any,
+        prob_any,
+        score_any,
+        conv_any,
+        taps_any,
+        bias_any,
+        g1_any,
+        gi_any,
+        g2_any,
+        dtb_any,
+        dlog_any,
+        skip_any,
+        z_any,
+        x_any,
+        b_any,
+        c_any,
+        dt_any,
+        ow_any,
+        eg_any,
+        eu_any,
+        ed_any,
+        st_any,
+        st,
+        out_ref,
+        fresh_ref,
         own_ref,
         ids_ref,
         prob_ref,
@@ -167,21 +226,6 @@
         dtb_ref,
         dlog_ref,
         skip_ref,
-        z_any,
-        x_any,
-        b_any,
-        c_any,
-        dt_any,
-        ow_any,
-        eg_any,
-        eu_any,
-        ed_any,
-        st_any,
-        out_ref,
-        sx_ref,
-        decx_ref,
-        bc_ref,
-        fresh_ref,
         hid,
         hbuf,
         hall,
@@ -196,11 +240,14 @@
         eg,
         eu,
         ed,
-        st,
         prod,
         fold,
+        grow,
         r0s,
         stepx,
+        decx,
+        sxs,
+        bcs,
         cpart,
         pre_out,
         pre_in,
@@ -208,6 +255,7 @@
         x_in,
         yown,
         ybuf,
+        igain,
         sel,
         bigh,
         bigl,
@@ -221,9 +269,11 @@
         o_in,
         wsem,
         gs,
-        gr,
+        hr,
+        yr,
         as_,
         ar,
+        pr,
     ) = refs
     rows, width = own_ref.shape
     cols = zw.shape[1]
@@ -235,12 +285,34 @@
     per = HEADS // SSM_GROUPS
     me = lax.axis_index("ep")
 
-    pairs = [(b_any, bw), (c_any, cw), (dt_any, dw)]
+    pairs = [
+        (own_any, own_ref),
+        (ids_any, ids_ref),
+        (g1_any, g1_ref),
+        (conv_any, conv_ref),
+        (taps_any, taps_ref),
+        (bias_any, bias_ref),
+        (dtb_any, dtb_ref),
+        (dlog_any, dlog_ref),
+        (skip_any, skip_ref),
+        (b_any, bw),
+        (c_any, cw),
+        (dt_any, dw),
+        (gi_any, gi_ref),
+        (g2_any, g2_ref),
+        (prob_any, prob_ref),
+        (score_any, score_ref),
+        (x_any, xw),
+        (z_any, zw),
+        (ow_any, ow),
+        (eg_any.at[0], eg),
+        (eu_any.at[0], eu),
+        (ed_any.at[0], ed),
+    ]
     pairs += [(st_any.at[t], st.at[t]) for t in range(rows)]
-    pairs += [(x_any, xw), (z_any, zw), (ow_any, ow)]
-    pairs += [(eg_any.at[0], eg), (eu_any.at[0], eu), (ed_any.at[0], ed)]
+    small, inputs, rest = 2, 12, 22
     loads = [pltpu.make_async_copy(src, dst, wsem.at[i]) for i, (src, dst) in enumerate(pairs)]
-    for load in loads:
+    for load in loads[:inputs] + loads[rest:] + loads[inputs:rest]:
         load.start()
 
     barrier = pltpu.get_barrier_semaphore()
@@ -248,6 +320,8 @@
         pl.semaphore_signal(
             barrier, inc=1, device_id=peer(lax.rem(me + d, n)), device_id_type=MESH
         )
+    for load in loads[:small]:
+        load.wait()
     ids = ids_ref[...].astype(F32)
     pick = iota((TOP, 128), 0)
     lane = iota((TOP, 128), 1)
@@ -259,10 +333,12 @@
     hid[...] = jnp.concatenate([own_ref[...].astype(F32), id_row], axis=0).astype(BF16)
     pl.semaphore_wait(barrier, n - 1)
 
-    hidden_ag = Gather(n, hbuf, gs.at[pl.ds(0, 1)], gr.at[pl.ds(0, n)])
+    hidden_ag = Gather(n, hbuf, gs.at[pl.ds(0, 1)], hr, direct=True)
     hidden_ag.start(hid)
     hbuf[me] = hid[...]
 
+    for load in loads[small:inputs]:
+        load.wait()
     gain1 = spread(g1_ref)
     own = hid[...].astype(F32)
     mine = rms_scale(own, gain1).astype(BF16)
@@ -272,8 +348,6 @@
     for k in range(held):
         summed = summed + conv_ref[k].astype(F32) * taps[k : k + 1]
     cpart[...] = jnp.concatenate([summed, jnp.zeros((ROWS - rows, summed.shape[1]), F32)], axis=0)
-    for load in loads[:3]:
-        load.wait()
     fresh_b = dot(mine, bw[...]).astype(BF16)
     fresh_c = dot(mine, cw[...]).astype(BF16)
     fresh_ref[:, INNER : INNER + SPAN] = fresh_b
@@ -285,8 +359,8 @@
     c_act = jax.nn.silu(
         cpart[:, INNER + SPAN :] + fresh_c.astype(F32) * taps[held : held + 1, INNER + SPAN :]
     )
-    bc_ref[:, :SPAN] = b_act
-    bc_ref[:, SPAN:] = c_act
+    bcs[:, :SPAN] = b_act
+    bcs[:, SPAN:] = c_act
     dt = dot_nt(mine, dw[...]).astype(BF16).astype(F32)
     step = jax.nn.softplus(dt + dtb_ref[...])
     dt_t = dot_nt(dw[...], mine).astype(BF16).astype(F32)
@@ -295,10 +369,10 @@
     for t in range(rows):
         at = slice(t * HEADS, (t + 1) * HEADS)
         stepx[at, :] = jnp.broadcast_to(step_t[:, t : t + 1], (HEADS, 128))
-        decx_ref[at, :] = jnp.broadcast_to(decay_t[:, t : t + 1], (HEADS, 128))
+        decx[at, :] = jnp.broadcast_to(decay_t[:, t : t + 1], (HEADS, 128))
     pad = slice(rows * HEADS, ROWS * HEADS)
     stepx[pad, :] = jnp.zeros(((ROWS - rows) * HEADS, 128), F32)
-    decx_ref[pad, :] = jnp.zeros(((ROWS - rows) * HEADS, 128), F32)
+    decx[pad, :] = jnp.zeros(((ROWS - rows) * HEADS, 128), F32)
     r0s[pad, :] = jnp.zeros(((ROWS - rows) * HEADS, 128), F32)
     bc = b_act * c_act
     bc_hi = bc.astype(BF16)
@@ -310,8 +384,6 @@
     coef = jnp.where(row_ok, coef, 0.0)
     coef = jnp.concatenate([coef, jnp.zeros((ROWS, 128 - HEADS), F32)], axis=1).astype(BF16)
 
-    hidden_ag.middle()
-
     def make_fold(i, carry):
         at = pl.ds(pl.multiple_of(i * 256, 256), 256)
         p_of = iota((256, 128), 0) // STATE + 4 * i
@@ -321,8 +393,8 @@
     lax.fori_loop(0, INNER // 256, make_fold, 0)
 
     def make_prod(t, carry):
-        pltpu.make_async_copy(st_any.at[t], st.at[t], wsem.at[3 + t]).wait()
-        row = bc_ref[pl.ds(t, 1), :]
+        pltpu.make_async_copy(st_any.at[t], st.at[t], wsem.at[rest + t]).wait()
+        row = bcs[pl.ds(t, 1), :]
         cs = []
         for g in range(SSM_GROUPS):
             c = row[:, SPAN + g * STATE : SPAN + (g + 1) * STATE]
@@ -335,8 +407,9 @@
         return carry
 
     lax.fori_loop(0, rows, make_prod, 0)
-    r0 = dot(prod[...], fold[...])
-    r0s[: rows * HEADS, :] = r0 * decx_ref[: rows * HEADS, :]
+    cut = (rows + 1) // 2 * HEADS
+    for at in (slice(0, cut), slice(cut, rows * HEADS)):
+        r0s[at, :] = dot(prod[at, :], fold[...]) * decx[at, :]
     low_half = iota((ROWS, 128), 1) < HEAD_DIM
     for m in range(INNER // 128):
         even = r0s[pl.ds(2 * m, ROWS, stride=HEADS), :]
@@ -348,17 +421,18 @@
         pre_out[j, :, 2 * cols :] = coef
     pre = Exchange(n, pre_out, pre_in, as_.at[pl.ds(0, 1)], ar.at[pl.ds(0, 1)])
     pre.start()
-
+    hidden_ag.middle()
     hidden_ag.last()
-    hidden_ag.finish()
+    for load in loads[inputs : inputs + 6]:
+        load.wait()
+    hidden_ag.finish(2)
+    hidden_ag.finish(3)
     for j in range(0, n, 2):
         at = slice(j * ROWS, (j + 2) * ROWS)
         pair = jnp.concatenate([hbuf[j].astype(F32), hbuf[j + 1].astype(F32)], axis=0)
         hall[at, :] = pair.astype(BF16)
         hg[at, :] = (pair * gain1).astype(BF16)
         hsq[at, :] = (pair * pair).astype(BF16)
-    for load in loads[3 + rows : 5 + rows]:
-        load.wait()
     ones = jnp.ones((width, 128), BF16)
     scale = lax.rsqrt(dot(hsq[...], ones) * (1.0 / width) + EPS)
     scale = jnp.concatenate([scale] * (cols // 128), axis=1)
@@ -394,11 +468,21 @@
             ys.append(readout * jax.nn.silu(zp[at]) * gain_cols)
         yown[j * ROWS : (j + 2) * ROWS, :] = jnp.concatenate(ys, axis=0).astype(BF16)
 
-    y_ag = Gather(n, ybuf, gs.at[pl.ds(1, 1)], gr.at[pl.ds(n, n)])
+    y_ag = Gather(n, ybuf, gs.at[pl.ds(1, 1)], yr, split=2)
     y_ag.start(yown)
-    back = Exchange(n, x_out, x_in, as_.at[pl.ds(1, 1)], ar.at[pl.ds(1, 1)])
-    back.start()
     ybuf[me] = yown[...]
+    igain[...] = jnp.broadcast_to(1.0 / gain_all, igain.shape)
+    ones_c = jnp.ones((cols, 128), BF16)
+
+    def project(blocks, acc, ssq):
+        for block in blocks:
+            lanes = pl.ds(pl.multiple_of(block * cols, 128), cols)
+            yb = ybuf[block]
+            acc = acc + dot(yb, ow[lanes, :])
+            inv = jnp.concatenate([igain[:, lanes]] * n, axis=0)
+            raw = yb.astype(F32) * inv
+            ssq = ssq + dot((raw * raw).astype(BF16), ones_c)
+        return acc, ssq
 
     q = iota((slots, total), 0)
     t_of = iota((slots, total), 1)
@@ -426,6 +510,11 @@
         ).astype(BF16)
 
     y_ag.middle()
+    near = [me] + [y_ag.near(d) for d in range(1, n // 4)]
+    acc = jnp.zeros((total, ncol), F32)
+    ssq = jnp.zeros((total, 128), F32)
+    loads[inputs + 6].wait()
+    acc, ssq = project(near, acc, ssq)
 
     span = chunks * cap
     wide = n * span
@@ -462,6 +551,23 @@
 
     y_ag.last()
 
+    back = Exchange(n, x_out, x_in, as_.at[pl.ds(1, 1)], ar.at[pl.ds(1, 1)])
+    back.start()
+    far = [y_ag.far(d) for d in range(n // 4)]
+    acc, ssq = project(far, acc, ssq)
+    shift = y_ag.mate - me
+    y_ag.finish(2)
+    acc, ssq = project([block + shift for block in near], acc, ssq)
+    y_ag.finish(3)
+    acc, ssq = project([block + shift for block in far], acc, ssq)
+    scale = lax.rsqrt(ssq * (1.0 / INNER) + EPS)
+    p = (acc * scale[:, :ncol]).astype(BF16)
+    picked = dot(sel[...], p).astype(BF16)
+    for e in range(n):
+        p_out[e] = picked[e * sp : e * sp + slots + ROWS]
+    p_ex = Exchange(n, p_out, p_in, as_.at[pl.ds(2, 1)], pr, planes=True)
+    p_ex.start()
+
     back.wait()
     for j in range(n):
         xv = x_in[j]
@@ -471,51 +577,37 @@
         for k in range(cols // 128):
             m = (j * cols) // 128 + k
             piece = xa[:, k * 128 : (k + 1) * 128]
-            sx_ref[pl.ds(2 * m, ROWS, stride=HEADS), :] = piece
-            sx_ref[pl.ds(2 * m + 1, ROWS, stride=HEADS), :] = pltpu.roll(piece, HEAD_DIM, 1)
-    sx_ref[...] = sx_ref[...] * stepx[...]
-
-    loads[5 + rows].wait()
-    y_ag.finish()
-    acc = jnp.zeros((total, ncol), F32)
-    ssq = jnp.zeros((total, 128), F32)
-    inv_gain = (1.0 / gain_all).astype(BF16)
-    ones_c = jnp.ones((cols, 128), BF16)
-    for j in range(n):
-        at = slice(j * cols, (j + 1) * cols)
-        yb = ybuf[j]
-        acc = acc + dot(yb, ow[at, :])
-        raw = yb * inv_gain[:, at]
-        ssq = ssq + dot(raw * raw, ones_c)
-    scale = lax.rsqrt(ssq * (1.0 / INNER) + EPS)
-    p = (acc * scale[:, :ncol]).astype(BF16)
-    picked = dot(sel[...], p).astype(BF16)
-    for e in range(n):
-        p_out[e] = picked[e * sp : e * sp + slots + ROWS]
-    p_ex = Exchange(n, p_out, p_in, as_.at[pl.ds(2, 1)], ar.at[pl.ds(2, 1)])
-    p_ex.start()
+            sxs[pl.ds(2 * m, ROWS, stride=HEADS), :] = piece
+            sxs[pl.ds(2 * m + 1, ROWS, stride=HEADS), :] = pltpu.roll(piece, HEAD_DIM, 1)
+    for load in loads[inputs + 7 : rest]:
+        load.wait()
+
     gain2 = spread(g2_ref)
-    for load in loads[6 + rows :]:
-        load.wait()
-    p_ex.wait()
     ssq = jnp.zeros((slots, 128), F32)
     ones_n = jnp.ones((ncol, 128), BF16)
-    mixed = []
-    for j in range(n):
-        at = slice(j * ncol, (j + 1) * ncol)
-        block = p_in[j].astype(F32)
+    band = 4 * ncol
+    units = eg.shape[1]
+    stage[:ROWS, :] = jnp.broadcast_to(gain2, (ROWS, width))
+    stage[ROWS:, :] = own
+    gate = jnp.zeros((slots, units), F32)
+    up = jnp.zeros((slots, units), F32)
+    for i, plane in enumerate(p_ex.order()):
+        p_ex.wait_plane(i, plane)
+        at = pl.ds(pl.multiple_of(plane * band, 128), band)
+        block = jnp.concatenate([p_in[4 * plane + w].astype(F32) for w in range(4)], axis=1)
         m = (hsel[:, at] + block[:slots]).astype(BF16).astype(F32)
-        mg[:, at] = (m * gain2[:, at]).astype(BF16)
-        ssq = ssq + dot((m * m).astype(BF16), ones_n)
-        mixed.append((own[:, at] + block[slots:]).astype(BF16).astype(F32))
-    mixed = jnp.concatenate(mixed, axis=1)
+        scaled = (m * stage[0:1, at]).astype(BF16)
+        square = (m * m).astype(BF16)
+        for w in range(4):
+            ssq = ssq + dot(square[:, w * ncol : (w + 1) * ncol], ones_n)
+        gate = gate + dot(scaled, eg[at, :])
+        up = up + dot(scaled, eu[at, :])
+        stage[ROWS:, at] = (stage[ROWS:, at] + block[slots:]).astype(BF16).astype(F32)
     scale = lax.rsqrt(ssq * (1.0 / width) + EPS)
     acts = []
-    for j in range(0, eg.shape[1], 128):
+    for j in range(0, units, 128):
         at = slice(j, j + 128)
-        gate = dot(mg[...], eg[:, at]) * scale
-        up = dot(mg[...], eu[:, at]) * scale
-        acts.append((jax.nn.silu(gate) * up).astype(BF16))
+        acts.append((jax.nn.silu(gate[:, at] * scale) * (up[:, at] * scale)).astype(BF16))
     act = jnp.concatenate(acts, axis=1)
     for k in range(0, chunks, 2):
         part = dot(act, ed[:, k * 128 : (k + 2) * 128])
@@ -528,6 +620,37 @@
         o_out[s] = spot_rows[s * span : (s + 1) * span, :].astype(BF16)
     o_ex = Exchange(n, o_out, o_in, as_.at[pl.ds(3, 1)], ar.at[pl.ds(3, 1)])
     o_ex.start()
+
+    def make_grow(i, carry):
+        at = pl.ds(pl.multiple_of(i * 256, 256), 256)
+        p_of = iota((128, 256), 1) // STATE + 4 * i
+        grow[:, at] = onehot(p_of == lax.rem(iota((128, 256), 0), HEAD_DIM))
+        return carry
+
+    lax.fori_loop(0, HEAD_DIM * STATE // 256, make_grow, 0)
+
+    def update(t, carry):
+        at = pl.ds(pl.multiple_of(t * HEADS, HEADS), HEADS)
+        sx = sxs[at, :] * stepx[at, :]
+        high = sx.astype(BF16).astype(F32)
+        low = pltpu.roll(sx - high, HEAD_DIM, 1)
+        lhs = jnp.where(iota((HEADS, 128), 1) < HEAD_DIM, high, low).astype(BF16)
+        dec = decx[at, :]
+        row = bcs[pl.ds(t, 1), :]
+        bs = []
+        for g in range(SSM_GROUPS):
+            b = row[:, g * STATE : (g + 1) * STATE]
+            bs.append(jnp.broadcast_to(jnp.concatenate([b, b], axis=1), (per, 2 * STATE)))
+        b_all = jnp.concatenate(bs, axis=0)
+        for k in range(HEAD_DIM * STATE // 256):
+            grown = dot(lhs, grow[:, k * 256 : (k + 1) * 256])
+            for i in range(2):
+                lanes = slice((2 * k + i) * 128, (2 * k + i + 1) * 128)
+                term = grown[:, i * 128 : (i + 1) * 128] * b_all
+                st[t, :, lanes] = dec * st[t, :, lanes] + term
+        return carry
+
+    lax.fori_loop(0, rows, update, 0)
     hidden_ag.drain()
     y_ag.drain()
     pre.drain()
@@ -538,7 +661,7 @@
     moe = dot(bigh[...], got) + dot(bigl[...], got)
     for k in range(chunks):
         at = slice(k * 128, (k + 1) * 128)
-        out_ref[:, at] = (mixed[:, at] + moe[k * ROWS : (k + 1) * ROWS])[:rows].astype(BF16)
+        out_ref[:, at] = (stage[ROWS:, at] + moe[k * ROWS : (k + 1) * ROWS])[:rows].astype(BF16)
     o_ex.drain()
 
 
@@ -561,15 +684,14 @@
     return pl.pallas_call(
         functools.partial(mixer_kernel, n, cap),
         out_shape=(
-            jax.ShapeDtypeStruct((rows, width), BF16),
-            jax.ShapeDtypeStruct((ROWS * HEADS, 128), F32),
-            jax.ShapeDtypeStruct((ROWS * HEADS, 128), F32),
-            jax.ShapeDtypeStruct((ROWS, 2 * SPAN), F32),
-            jax.ShapeDtypeStruct((ROWS, INNER + 2 * SPAN), BF16),
+            pltpu.VMEM((rows, HEADS, HEAD_DIM * STATE), F32),
+            pltpu.VMEM((rows, width), BF16),
+            pltpu.VMEM((ROWS, INNER + 2 * SPAN), BF16),
         ),
-        in_specs=[vm] * 13 + [hbm] * 10,
-        out_specs=(vm,) * 5,
-        scratch_shapes=[
+        in_specs=[hbm] * 23,
+        out_specs=(vm,) * 3,
+        scratch_shapes=[pltpu.VMEM(x.shape, x.dtype) for x in args[:13]]
+        + [
             buf(ROWS, width),
             buf(n, ROWS, width),
             buf(total, width),
@@ -584,11 +706,14 @@
             buf(width, units),
             buf(width, units),
             buf(units, width),
-            buf(rows, HEADS, HEAD_DIM * STATE, dtype=F32),
             buf(rows * HEADS, HEAD_DIM * STATE),
             buf(INNER, 128),
+            buf(128, HEAD_DIM * STATE),
             buf(ROWS * HEADS, 128, dtype=F32),
             buf(ROWS * HEADS, 128, dtype=F32),
+            buf(ROWS * HEADS, 128, dtype=F32),
+            buf(ROWS * HEADS, 128, dtype=F32),
+            buf(ROWS, 2 * SPAN, dtype=F32),
             buf(ROWS, INNER + 2 * SPAN, dtype=F32),
             buf(n, ROWS, 2 * cols + 128),
             buf(n, ROWS, 2 * cols + 128),
@@ -596,6 +721,7 @@
             buf(n, ROWS, cols),
             buf(total, cols),
             buf(n, total, cols),
+            buf(ROWS, INNER, dtype=F32),
             buf(n * sp, total),
             buf(chunks * ROWS, n * span),
             buf(chunks * ROWS, n * span),
@@ -607,83 +733,57 @@
             buf(n * span, 128, dtype=F32),
             buf(n, span, 128),
             buf(n, span, 128),
-            dma((9 + rows,)),
+            dma((22 + rows,)),
             dma((2,)),
+            dma((n,)),
             dma((2 * n,)),
             dma((4,)),
             dma((4,)),
+            dma((n // 4,)),
         ],
         compiler_params=pltpu.CompilerParams(
-            collective_id=0, has_side_effects=True, vmem_limit_bytes=56 << 20
+            collective_id=0, has_side_effects=True, vmem_limit_bytes=48 << 20
         ),
         name="mixer",
     )(*args)
 
 
-def state_kernel(
-    sx_ref, dec_ref, bc_ref, fresh_ref, conv_ref, layer_ref, st_ref, out_ref, conv_out, lay, e_ref
-):
-    s = pl.program_id(0)
+def write_kernel(st_ref, layer_ref, fresh_ref, conv_ref, out_any, lay_any, conv_any, rows3, sem):
     rows = layer_ref.shape[0]
-    blocks = HEAD_DIM * STATE // 256
-
-    @pl.when(s == 0)
-    def _():
-        held = conv_ref.shape[0]
-        for k in range(1, held):
-            conv_out[k - 1] = conv_ref[k]
-        conv_out[held - 1] = fresh_ref[...][:rows]
-        lay[...] = layer_ref[...]
-
-        def make(k, carry):
-            at = pl.ds(pl.multiple_of(k * 256, 256), 256)
-            p_of = iota((128, 256), 1) // STATE + 4 * k
-            e_ref[:, at] = onehot(p_of == lax.rem(iota((128, 256), 0), HEAD_DIM))
-            return carry
-
-        lax.fori_loop(0, blocks, make, 0)
-
-    sx = sx_ref[...]
-    high = sx.astype(BF16).astype(F32)
-    low = pltpu.roll(sx - high, HEAD_DIM, 1)
-    lhs = jnp.where(iota((HEADS, 128), 1) < HEAD_DIM, high, low).astype(BF16)
-    dec = dec_ref[...]
-    row = bc_ref[pl.ds(s, 1), :]
-    per = HEADS // SSM_GROUPS
-    bs = []
-    for g in range(SSM_GROUPS):
-        b = row[:, g * STATE : (g + 1) * STATE]
-        bs.append(jnp.broadcast_to(jnp.concatenate([b, b], axis=1), (per, 2 * STATE)))
-    b_all = jnp.concatenate(bs, axis=0)
-    for k in range(blocks):
-        grown = dot(lhs, e_ref[:, k * 256 : (k + 1) * 256])
-        for i in range(2):
-            at = slice((2 * k + i) * 128, (2 * k + i + 1) * 128)
-            out_ref[0, :, at] = dec * st_ref[0, :, at] + grown[:, i * 128 : (i + 1) * 128] * b_all
-
-
-def state_update(sx, dec, bc, fresh, conv_t, layer, state_in):
-    rows, _, flat = state_in.shape
-
-    def whole(x):
-        return pl.BlockSpec(x.shape, lambda s: (0,) * len(x.shape))
-
-    part = pl.BlockSpec((HEADS, 128), lambda s: (s, 0))
-    block = pl.BlockSpec((1, HEADS, flat), lambda s: (s, 0, 0))
+    held = conv_ref.shape[0]
+    copies = [pltpu.make_async_copy(st_ref.at[t], out_any.at[t], sem.at[t]) for t in range(rows)]
+    copies.append(pltpu.make_async_copy(layer_ref, lay_any, sem.at[rows]))
+    for copy in copies:
+        copy.start()
+    for k in range(1, held):
+        rows3[k - 1] = conv_ref[k]
+    rows3[held - 1] = fresh_ref[...][:rows]
+    copies.append(pltpu.make_async_copy(rows3, conv_any, sem.at[rows + 1]))
+    copies[-1].start()
+    for copy in copies:
+        copy.wait()
+
+
+def write(st, layer, fresh, conv_t):
+    rows = layer.shape[0]
+    vm = pl.BlockSpec(memory_space=pltpu.VMEM)
+    hbm = pl.BlockSpec(memory_space=pl.ANY)
     return pl.pallas_call(
-        state_kernel,
-        grid=(rows,),
+        write_kernel,
         out_shape=(
-            jax.ShapeDtypeStruct(state_in.shape, F32),
+            jax.ShapeDtypeStruct(st.shape, F32),
+            jax.ShapeDtypeStruct(layer.shape, BF16),
             jax.ShapeDtypeStruct(conv_t.shape, BF16),
-            jax.ShapeDtypeStruct(layer.shape, BF16),
         ),
-        in_specs=[part, part, whole(bc), whole(fresh), whole(conv_t), whole(layer), block],
-        out_specs=(block, whole(conv_t), whole(layer)),
-        scratch_shapes=[pltpu.VMEM((128, flat), BF16)],
-        compiler_params=pltpu.CompilerParams(vmem_limit_bytes=24 << 20),
-        name="state",
-    )(sx, dec, bc, fresh, conv_t, layer, state_in)
+        in_specs=[vm] * 4,
+        out_specs=(hbm,) * 3,
+        scratch_shapes=[
+            pltpu.VMEM(conv_t.shape, BF16),
+            pltpu.SemaphoreType.DMA((rows + 2,)),
+        ],
+        compiler_params=pltpu.CompilerParams(vmem_limit_bytes=4 << 20),
+        name="write",
+    )(st, layer, fresh, conv_t)
 
 
 def body(
@@ -740,10 +840,10 @@
         expert_down,
         state_in,
     )
-    layer, sx, dec, bc, fresh = mixer(
+    st, layer, fresh = mixer(
         n, cap, args, rows, width, z_weight, out_weight, expert_gate, expert_down
     )
-    state_out, conv_out, layer_out = state_update(sx, dec, bc, fresh, conv_t, layer, state_in)
+    state_out, layer_out, conv_out = write(st, layer, fresh, conv_t)
     return (layer_out, state_out, conv_out.transpose(1, 0, 2))
 
 

time: 61.1 us -> 48.4 us (0.79)
  Pallas kernels: 55.8 us -> 47.6 us
  local copies, waits for them, and re-layouts: 4.26 us -> 0.01 us
    pallas_call x2, Pallas kernels: 55.8 us -> 47.6 us  [the longest x1 44.5 us: mixer(): pl.pallas_call(functools.partial(mixer_kernel, n, cap), out_shape=(pltpu....]
    unnamed x16 -> x2, local copies, waits for them, and re-layouts: 4.26 us -> 0.01 us
where the time goes in v2:
time: 48.4 us; the launch traced here: 48.2 us
  Pallas kernels  47.6 us (98%)
  between operations  0.66 us (1%)
    pallas_call x1, Pallas kernels, mixer(): pl.pallas_call(functools.partial(mixer_kernel, n, cap), out_shape=(pltpu....  44.5 us
    pallas_call x1, Pallas kernels, write(): pl.pallas_call(write_kernel, out_shape=(jax.ShapeDtypeStruct(st.shape, F3...  3.1 us

profile of v2, /device:TPU:0, one launch (start us, length us, event | category | flops | bytes accessed | tf_op | source)
XLA Modules:
  0.0 48.2 jit_solution(2870085172126706486)
XLA Ops:
  0.6 0.0 copy-start
  0.7 44.5 %mixer.1 = (f32[7,64,4096]{2,1,0:T(8,128)S(1)}, bf16[7,2048]{1,0:T(8,128)(2,1)S(1)}, bf16[8,4608]{1,0:T(8,128)(2,1)S(1)}) custom-call(bf16[7,2048]{1,0:T(8,128)(2,1)} %refs_0_.1, s32[4,7]{1,0:T(4,128)} %bitcast.20, f32[1,7]{1,0:T(1,128)} %bitcast.22, f32[4,7]{1,0:T(4,128)} %bitcast.21, bf16[3,7,4608]{2,1,0:T(8,128)(2,1)} %bitcast.13, ...), custom_call_target="tpu_custom_call" | custom-call | tf_op jit(solution)/shard_map/mixer/pallas_call | solution.py:684
  45.1 0.0 copy-done
  45.1 3.1 %write.1 = (f32[7,64,4096]{2,1,0:T(8,128)}, bf16[7,2048]{1,0:T(8,128)(2,1)}, bf16[3,7,4608]{2,1,0:T(8,128)(2,1)}) custom-call(f32[7,64,4096]{2,1,0:T(8,128)S(1)} %get-tuple-element.9.st_ref, bf16[7,2048]{1,0:T(8,128)(2,1)S(1)} %get-tuple-element.10.layer_ref, bf16[8,4608]{1,0:T(8,128)(2,1)S(1)} %get-tuple-element.11.fresh_ref, bf16[3,7,4608]{2,1,0:T(8,128)(2,1)S(1)} %bitcast.14), custom_call_target="tpu_custom_call" | custom-call | tf_op jit(solution)/shard_map/write/pallas_call | solution.py:771
Async XLA Ops:
  0.6 44.5 %copy-start = (bf16[7,3,4608]{2,0,1:T(8,128)(2,1)S(1)}, bf16[7,3,4608]{2,0,1:T(8,128)(2,1)}, u32[]{:S(2)}) copy-start(bf16[7,3,4608]{2,0,1:T(8,128)(2,1)} %param.25) | copy-start | bytes 580612
